TPU v7x, 512 devices: a whole 4x8x8 slice. The times are simulated.
512 devices in a mesh: ep: 128 (over z, y, core), tp: 4 (over x).
Axes of the slice: x: 4, y: 8, z: 8, core: 2. Of those that a mesh axis runs over, the one named last changes fastest.
Arguments:
- tokens: bfloat16 [2048, 1024], P(('ep', 'tp')), may hold values from -6 to 6
- lengths: int32 [2048], P(('ep', 'tp')), may hold values from 256 to 1024, as said below
- cache_latent: bfloat16 [2048, 1024, 256], P(('ep', 'tp')), may hold values from -160 to 160
- cache_rope: bfloat16 [2048, 32, 1024], P(('ep', 'tp')), may hold values from -6 to 6
- attn_gain: float32 [1024], replicated, may hold values from 0.1 to 1.9
- latent_gain: float32 [256], replicated, may hold values from 0.1 to 1.9
- post_gain: float32 [1024], replicated, may hold values from 0.1 to 1.9
- ffn_gain: float32 [1024], replicated, may hold values from 0.1 to 1.9
- out_gain: float32 [1024], replicated, may hold values from 0.1 to 1.9
- w_latent: bfloat16 [1024, 256], P(None, 'tp'), may hold values from -0.1875 to 0.1875
- w_rope_key: bfloat16 [1024, 32], replicated, may hold values from -0.1875 to 0.1875
- w_query: bfloat16 [1024, 768], P(None, 'tp'), may hold values from -0.1875 to 0.1875
- w_absorb_key: bfloat16 [8, 64, 256], P('tp'), may hold values from -0.75 to 0.75
- w_absorb_value: bfloat16 [8, 256, 64], P('tp'), may hold values from -0.375 to 0.375
- w_out: bfloat16 [512, 1024], P('tp'), may hold values from -0.25 to 0.25
- routes: int32 [2048, 6], P(('ep', 'tp')), may hold values from 0 to 127, all different within a row; in each aligned block of 16 rows (0 to 15, 16 to 31, ...) at most 2 rows name the same one
- route_weights: float32 [2048, 6], P(('ep', 'tp')), may hold values from 0.2 to 1
- w_exp_gate: bfloat16 [128, 1024, 256], P('ep'), may hold values from -0.1875 to 0.1875
- w_exp_up: bfloat16 [128, 1024, 256], P('ep'), may hold values from -0.1875 to 0.1875
- w_exp_down: bfloat16 [128, 256, 1024], P('ep'), may hold values from -0.375 to 0.375
- w_dense_gate: bfloat16 [4096, 1024], P('ep'), may hold values from -0.1875 to 0.1875
- w_dense_up: bfloat16 [4096, 1024], P('ep'), may hold values from -0.1875 to 0.1875
- w_dense_down: bfloat16 [4096, 1024], P('ep'), may hold values from -0.09375 to 0.09375
- dense_gate_vector: float32 [1024], replicated, may hold values from -0.1875 to 0.1875
Outputs:
- output: bfloat16 [2048, 1024], P(('ep', 'tp'))
- new_latent: bfloat16 [2048, 256], P(('ep', 'tp'))
- new_rope_key: bfloat16 [2048, 32], P(('ep', 'tp'))
Inputs may be any that keep to these rules, and one draw needn't show every extreme that they name: `routes`: in each aligned block of 16 rows no expert is named by more than 2 rows; each row names 6 different experts. `lengths`: some sequence holds exactly 1024 cached positions.
All inputs are finite; a program needn't handle non-finite values.
Results may differ from a plain program's by a relative error of at most 0.015.
Values may be sent and summed in bfloat16 or wider, within the bound.
A program may use at most 64 MiB of HBM per device.

v0:
```python
import jax
import jax.numpy as jnp
from jax import lax
from jax.sharding import Mesh
from jax.sharding import PartitionSpec as P

EP = ("ep_0", "ep_1", "ep_2")
EP_TP = ("ep_0", "ep_1", "ep_2", "tp")


epsilon = 1e-06
rope_base = 10000.0
negative = -1e30


def copy_for_each(shard, axis):
    copies = jnp.broadcast_to(shard, (lax.axis_size(axis), *shard.shape))
    return lax.all_to_all(copies, axis, split_axis=0, concat_axis=0, tiled=True)


def laid_out(parts, dim):
    dims = list(parts.shape[1:])
    dims[dim] *= parts.shape[0]
    return jnp.moveaxis(parts, 0, dim).reshape(dims)


def collect(shard, axis, dim):
    parts = copy_for_each(shard, axis)
    return laid_out(parts, dim)


def sent_together(arrays, axis, split_dim, concat_dim, along):
    widths = [a.shape[along] for a in arrays]
    both = jnp.concatenate(arrays, axis=along)
    result = lax.all_to_all(both, axis, split_axis=split_dim, concat_axis=concat_dim, tiled=True)
    return tuple(jnp.split(result, [sum(widths[:k]) for k in range(1, len(widths))], axis=along))


def cut_along(shard, dim, devices):
    before, after = (shard.shape[:dim], shard.shape[dim + 1 :])
    return jnp.moveaxis(shard.reshape(*before, devices, -1, *after), dim, 0)


def sent_and_summed(shard, axis, dim):
    parts = cut_along(shard, dim, lax.axis_size(axis))
    arrived = lax.all_to_all(parts, axis, split_axis=0, concat_axis=0, tiled=True)
    return arrived.astype(jnp.float32).sum(axis=0)


def gather_axes(shard, axes, dim):
    far, near = axes
    first = copy_for_each(shard, far)
    parts = jnp.swapaxes(copy_for_each(first, near), 0, 1)
    return laid_out(parts.reshape(-1, *shard.shape), dim)


def summed_rows(shard, axes, dim):
    far, near = axes
    own = sent_and_summed(cut_along(shard, dim, lax.axis_size(far)), near, dim + 1)
    return jnp.sum(
        lax.all_to_all(own.astype(jnp.bfloat16), far, 0, 0, tiled=True).astype(jnp.float32), axis=0
    )


def normalize(values, gain_vec):
    values = values.astype(jnp.float32)
    return (
        values * lax.rsqrt(jnp.mean(values * values, axis=-1, keepdims=True) + epsilon) * gain_vec
    )


def rotate(values, positions):
    half_width = values.shape[-1] // 2
    inverse = rope_base ** (-jnp.arange(half_width, dtype=jnp.float32) / half_width)
    angles = positions.astype(jnp.float32)[..., None] * inverse
    cosine = jnp.cos(angles)
    sine_part = jnp.sin(angles)
    first_half = values[..., :half_width]
    second = values[..., half_width:]
    return jnp.concatenate(
        [first_half * cosine - second * sine_part, first_half * sine_part + second * cosine],
        axis=-1,
    )


def attend(q_latent, q_rope, cache_lat, cache_rot, new_lat, new_rot, seq_lengths, scaling):
    scores = jnp.einsum("shc,slc->shl", q_latent, cache_lat, preferred_element_type=jnp.float32)
    scores = scores + jnp.einsum(
        "shr,srl->shl", q_rope, cache_rot, preferred_element_type=jnp.float32
    )
    scores = scores * scaling
    own_score = jnp.sum(
        q_latent.astype(jnp.float32) * new_lat.astype(jnp.float32)[:, None, :], axis=-1
    )
    own_score = (
        own_score
        + jnp.sum(q_rope.astype(jnp.float32) * new_rot.astype(jnp.float32)[:, None, :], axis=-1)
    ) * scaling
    visible = (
        jnp.arange(cache_lat.shape[1], dtype=jnp.int32)[None, None, :] < seq_lengths[:, None, None]
    )
    scores = jnp.where(visible, scores, negative)
    row_max = jnp.maximum(jnp.max(scores, axis=-1), own_score)
    weights = jnp.exp(scores - row_max[..., None])
    own_weight = jnp.exp(own_score - row_max)
    totals = jnp.sum(weights, axis=-1) + own_weight
    probabilities = (weights / totals[..., None]).astype(jnp.bfloat16)
    own_prob = (own_weight / totals).astype(jnp.bfloat16)
    mixed = jnp.einsum("shl,slc->shc", probabilities, cache_lat, preferred_element_type=jnp.float32)
    mixed = (
        mixed + own_prob.astype(jnp.float32)[..., None] * new_lat.astype(jnp.float32)[:, None, :]
    )
    return mixed.astype(jnp.bfloat16)


def expert_rows(rows_in, gate_w, up_w, down_w):
    model_width = rows_in.shape[-1]
    flattened = rows_in.reshape(-1, model_width)
    gate_pre = jnp.dot(flattened, gate_w, preferred_element_type=jnp.float32)
    up_proj = jnp.dot(flattened, up_w, preferred_element_type=jnp.float32)
    activity = (jax.nn.silu(gate_pre) * up_proj).astype(jnp.bfloat16)
    result = jnp.dot(activity, down_w, preferred_element_type=jnp.float32).astype(jnp.bfloat16)
    return result.reshape(rows_in.shape)


def rank_in_expert(flattened, experts):
    route_count = flattened.shape[0]
    onehot = (flattened[:, None] == jnp.arange(experts, dtype=jnp.int32)[None, :]).astype(
        jnp.float32
    )
    strictly = (jnp.arange(route_count)[:, None] > jnp.arange(route_count)[None, :]).astype(
        jnp.float32
    )
    earlier = jnp.dot(strictly, onehot, precision=lax.Precision.HIGHEST)
    return jnp.sum(earlier * onehot, axis=1).astype(jnp.int32)


def shards(
    tokens,
    lengths,
    cache_latent,
    cache_rope,
    attn_gain,
    latent_gain,
    post_gain,
    ffn_gain,
    out_gain,
    w_latent,
    w_rope_key,
    w_query,
    w_absorb_key,
    w_absorb_value,
    w_out,
    routes,
    route_weights,
    w_exp_gate,
    w_exp_up,
    w_exp_down,
    w_dense_gate,
    w_dense_up,
    w_dense_down,
    dense_gate_vector,
):
    own_rows = tokens.shape[0]
    model_width = tokens.shape[1]
    tp_count = lax.axis_size("tp")
    ep_count = lax.axis_size(EP)
    rope_width = w_rope_key.shape[1]
    nope_width = w_absorb_key.shape[1]
    head_span = nope_width + rope_width
    scaling = head_span ** (-0.5)
    top_count = routes.shape[1]
    group_size = own_rows * tp_count
    capacity = min(
        group_size, max(2, (3 * group_size * top_count + 2 * ep_count - 1) // (2 * ep_count))
    )
    hidden = normalize(tokens, attn_gain).astype(jnp.bfloat16)
    new_rope_key = rotate(
        jnp.dot(hidden, w_rope_key, preferred_element_type=jnp.float32), lengths
    ).astype(jnp.bfloat16)
    local_heads = w_absorb_key.shape[0]
    group_hidden = collect(hidden, "tp", 0)
    latent_part = jnp.dot(group_hidden, w_latent, preferred_element_type=jnp.float32)
    latent_full = lax.all_to_all(latent_part, "tp", split_axis=0, concat_axis=1, tiled=True)
    new_latent = normalize(latent_full, latent_gain).astype(jnp.bfloat16)
    queries = jnp.dot(group_hidden, w_query, preferred_element_type=jnp.float32).astype(
        jnp.bfloat16
    )
    queries = queries.reshape(group_size, local_heads, head_span)
    query_latent = jnp.einsum(
        "shn,hnc->shc", queries[..., :nope_width], w_absorb_key, preferred_element_type=jnp.float32
    ).astype(jnp.bfloat16)
    query_latent, query_rope = sent_together(
        (query_latent, queries[..., nope_width:]), "tp", 0, 1, 2
    )
    query_rope = rotate(query_rope.astype(jnp.float32), lengths[:, None]).astype(jnp.bfloat16)
    attended = attend(
        query_latent,
        query_rope,
        cache_latent,
        cache_rope,
        new_latent,
        new_rope_key,
        lengths,
        scaling,
    )
    attended = lax.all_to_all(attended, "tp", split_axis=1, concat_axis=0, tiled=True)
    head_out = (
        jnp.einsum("shc,hcv->shv", attended, w_absorb_value, preferred_element_type=jnp.float32)
        .astype(jnp.bfloat16)
        .reshape(group_size, -1)
    )
    mixed = sent_and_summed(
        jnp.dot(head_out, w_out, preferred_element_type=jnp.float32).astype(jnp.bfloat16), "tp", 0
    )
    residual = (tokens.astype(jnp.float32) + normalize(mixed, post_gain)).astype(jnp.bfloat16)
    ffn_in = normalize(residual, ffn_gain).astype(jnp.bfloat16)
    gate_w = w_exp_gate[0]
    up_w = w_exp_up[0]
    down_w = w_exp_down[0]
    flattened = routes.reshape(-1)
    order_rank = rank_in_expert(flattened, ep_count)
    slot_index = (flattened * capacity + order_rank).reshape(own_rows, top_count)
    dispatch = jnp.any(
        slot_index[None, :, :] == jnp.arange(ep_count * capacity, dtype=jnp.int32)[:, None, None],
        axis=-1,
    ).astype(jnp.bfloat16)
    outgoing = jnp.dot(dispatch, ffn_in, preferred_element_type=jnp.float32).astype(jnp.bfloat16)
    outgoing = outgoing.reshape(ep_count, capacity, model_width)
    result = expert_rows(
        lax.all_to_all(outgoing, EP, split_axis=0, concat_axis=0, tiled=True), gate_w, up_w, down_w
    )
    returned = lax.all_to_all(result, EP, split_axis=0, concat_axis=0, tiled=True)
    picked = returned.reshape(ep_count * capacity, model_width)[slot_index].astype(jnp.float32)
    routed = jnp.sum(route_weights[..., None] * picked, axis=1)
    piece_rows = gather_axes(ffn_in, (("ep_0", "ep_1"), "ep_2"), 0)
    dims = (((1,), (1,)), ((), ()))
    gate_pre = lax.dot_general(piece_rows, w_dense_gate, dims, preferred_element_type=jnp.float32)
    up_proj = lax.dot_general(piece_rows, w_dense_up, dims, preferred_element_type=jnp.float32)
    dense_act = (jax.nn.silu(gate_pre) * up_proj).astype(jnp.bfloat16)
    dense_out = summed_rows(
        jnp.dot(dense_act, w_dense_down, preferred_element_type=jnp.float32).astype(jnp.bfloat16),
        (("ep_0", "ep_1"), "ep_2"),
        0,
    )
    dense_gate = jax.nn.sigmoid(jnp.sum(ffn_in.astype(jnp.float32) * dense_gate_vector, axis=-1))
    combined = routed + dense_gate[:, None] * dense_out
    output = (residual.astype(jnp.float32) + normalize(combined, out_gain)).astype(jnp.bfloat16)
    return (output, new_latent, new_rope_key)


def solution(mesh):
    torus = Mesh(mesh.devices.reshape(8, 8, 2, mesh.shape["tp"]), ("ep_0", "ep_1", "ep_2", "tp"))
    placed = (
        P(EP_TP, None),
        P(EP_TP),
        P(EP_TP, None, None),
        P(EP_TP, None, None),
        P(),
        P(),
        P(),
        P(),
        P(),
        P(None, "tp"),
        P(),
        P(None, "tp"),
        P("tp", None, None),
        P("tp", None, None),
        P("tp", None),
        P(EP_TP, None),
        P(EP_TP, None),
        P(EP, None, None),
        P(EP, None, None),
        P(EP, None, None),
        P(EP, None),
        P(EP, None),
        P(EP, None),
        P(),
    )
    return jax.shard_map(
        shards,
        mesh=torus,
        in_specs=placed,
        out_specs=(P(EP_TP, None), P(EP_TP, None), P(EP_TP, None)),
        check_vma=False,
    )
```

profile of v0, /device:TPU:1, one launch (start us, length us, event | category | flops | bytes accessed | tf_op | source)
XLA Modules:
  0.0 182.5 jit_solution(13544683477178104833)
XLA Ops:
  0.7 1.0 fusion.31
  3.0 4.8 %all-to-all-start = ((bf16[4,4,1024]{2,1,0:T(4,128)(2,1)}), bf16[4,4,1024]{2,1,0:T(4,128)(2,1)S(1)}, u32[]{:S(2)}, u32[]{:S(2)}) async-start(bf16[4,4,1024]{2,1,0:T(4,128)(2,1)} %broadcast_in_dim.17), calls=%async_computation | async-start | bytes 65536 | tf_op jit(solution)/shard_map/all_to_all | solution.py:18
  11.0 1.2 all-to-all-done
  12.2 1.2 convolution_convert_fusion.6
  13.6 1.1 fusion.18
  15.3 3.2 %all-to-all-start.2 = ((f32[4,1,256]{2,1,0:T(1,128)}), f32[4,1,256]{2,1,0:T(1,128)S(1)}, u32[]{:S(2)}, u32[]{:S(2)}) async-start(f32[4,1,256]{2,1,0:T(1,128)} %reshape.286), calls=%async_computation.2 | async-start | bytes 8192 | tf_op jit(solution)/shard_map/all_to_all | solution.py:184
  20.2 2.5 %all-to-all-done.2 = f32[4,1,256]{2,1,0:T(1,128)S(1)} async-done(((f32[4,1,256]{2,1,0:T(1,128)}), f32[4,1,256]{2,1,0:T(1,128)S(1)}, u32[]{:S(2)}, u32[]{:S(2)}) %all-to-all-start.2) | async-done | bytes 4128 | tf_op jit(solution)/shard_map/all_to_all | solution.py:184
  22.7 3.3 %all-to-all-start.1 = ((bf16[16,2,288]{2,1,0:T(2,128)(2,1)}), bf16[16,2,288]{2,1,0:T(2,128)(2,1)S(1)}, u32[]{:S(2)}, u32[]{:S(2)}) async-start(bf16[16,2,288]{2,1,0:T(2,128)(2,1)} %copy.72), calls=%async_computation.1 | async-start | bytes 49152 | tf_op jit(solution)/shard_map/all_to_all | solution.py:35
  27.4 1.3 fusion.52
  28.8 1.4 all-to-all-done.1
  32.3 6.8 %all_to_all.92 = bf16[4,8,256]{2,0,1:T(4,128)(2,1)S(1)} all-to-all(bf16[4,8,256]{2,0,1:T(4,128)(2,1)S(1)} %copy.75), channel_id=1, replica_groups=mesh['ep_0'=8,'ep_1'=8,'ep_2'=2,'tp'=4] {'tp'}, dimensions={1} | all-to-all | bytes 32768 | tf_op jit(solution)/shard_map/all_to_all | solution.py:207
  39.5 6.7 %all_to_all.93 = bf16[4,4,1024]{2,1,0:T(4,128)(2,1)S(1)} all-to-all(bf16[4,4,1024]{2,1,0:T(4,128)(2,1)S(1)} %reshape.269), channel_id=1, replica_groups=mesh['ep_0'=8,'ep_1'=8,'ep_2'=2,'tp'=4] {'tp'}, dimensions={0} | all-to-all | bytes 65536 | tf_op jit(solution)/shard_map/all_to_all | solution.py:46
  47.7 16.3 %all-to-all-start.7 = ((bf16[64,4,1024]{2,1,0:T(4,128)(2,1)}), bf16[64,4,1024]{2,1,0:T(4,128)(2,1)S(1)}, u32[]{:S(2)}, u32[]{:S(2)}) async-start(bf16[64,4,1024]{2,1,0:T(4,128)(2,1)} %broadcast_in_dim.24), calls=%async_computation.7 | async-start | bytes 1048576 | tf_op jit(solution)/shard_map/all_to_all | solution.py:18
  65.1 1.0 reshape.270
  66.1 12.3 %all-to-all-done.7 = bf16[64,4,1024]{2,1,0:T(4,128)(2,1)S(1)} async-done(((bf16[64,4,1024]{2,1,0:T(4,128)(2,1)}), bf16[64,4,1024]{2,1,0:T(4,128)(2,1)S(1)}, u32[]{:S(2)}, u32[]{:S(2)}) %all-to-all-start.7) | async-done | bytes 524320 | tf_op jit(solution)/shard_map/all_to_all | solution.py:18
  78.7 12.1 %all_to_all.94 = bf16[2,64,4,1024]{3,2,1,0:T(4,128)(2,1)S(1)} all-to-all(bf16[2,64,4,1024]{3,2,1,0:T(4,128)(2,1)S(1)} %broadcast_in_dim.25), channel_id=1, replica_groups=mesh['ep_0'=8,'ep_1'=8,'ep_2'=2,'tp'=4] {'ep_2'}, dimensions={0} | all-to-all | bytes 2097152 | tf_op jit(solution)/shard_map/all_to_all | solution.py:18
  90.8 1.6 copy.79
  92.4 1.4 reshape_reshape.6
  94.2 1.9 %convolution_convert_fusion = bf16[512,1024]{1,0:T(8,128)(2,1)} fusion(bf16[32,1024]{1,0:T(8,128)(2,1)S(1)} %copy-done.5, bf16[512,1024]{1,0:T(8,128)(2,1)S(1)} %reshape_reshape.6, bf16[32,1024]{1,0:T(8,128)(2,1)S(1)} %copy-done.6, f32[512,32]{0,1:T(8,128)S(1)} %fusion.55), kind=kOutput, calls=%fused_computation.1 | convolution fusion | flops 67731456 | bytes 2293760 | tf_op jit(solution)/shard_map/dot_general | solution.py:242
  96.1 1.5 reshape_reshape.7
  97.9 4.6 %all_to_all.95 = bf16[2,64,4,1024]{3,2,1,0:T(4,128)(2,1)S(1)} all-to-all(bf16[2,64,4,1024]{3,2,1,0:T(4,128)(2,1)S(1)} %bitcast.57), channel_id=1, replica_groups=mesh['ep_0'=8,'ep_1'=8,'ep_2'=2,'tp'=4] {'ep_2'}, dimensions={0} | all-to-all | bytes 2097152 | tf_op jit(solution)/shard_map/all_to_all | solution.py:46
  102.5 6.6 %all-to-all-start.5 = ((bf16[128,2,1024]{2,1,0:T(2,128)(2,1)}), bf16[128,2,1024]{2,1,0:T(2,128)(2,1)}, u32[]{:S(2)}, u32[]{:S(2)}) async-start(bf16[128,2,1024]{2,1,0:T(2,128)(2,1)} %reshape.270), calls=%async_computation.5 | async-start | bytes 1048576 | tf_op jit(solution)/shard_map/all_to_all | solution.py:231
  109.1 1.9 %reduce_sum.140 = bf16[64,4,1024]{2,1,0:T(4,128)(2,1)} reduce(bf16[2,64,4,1024]{3,2,1,0:T(4,128)(2,1)S(1)} %all_to_all.95, bf16[]{:T(256)} %constant.41.clone.1), dimensions={0}, to_apply=%region_13.14 | reduce | flops 262144 | bytes 1572866 | tf_op jit(solution)/shard_map/reduce_sum | solution.py:47
  111.0 18.4 %all-to-all-done.5 = bf16[128,2,1024]{2,1,0:T(2,128)(2,1)} async-done(((bf16[128,2,1024]{2,1,0:T(2,128)(2,1)}), bf16[128,2,1024]{2,1,0:T(2,128)(2,1)}, u32[]{:S(2)}, u32[]{:S(2)}) %all-to-all-start.5) | async-done | bytes 524320 | tf_op jit(solution)/shard_map/all_to_all | solution.py:231
  129.4 4.8 %all-to-all-start.10 = ((bf16[64,4,1024]{2,1,0:T(4,128)(2,1)}), bf16[64,4,1024]{2,1,0:T(4,128)(2,1)S(1)}, u32[]{:S(2)}, u32[]{:S(2)}) async-start(bf16[64,4,1024]{2,1,0:T(4,128)(2,1)} %reduce_sum.140), calls=%async_computation.10 | async-start | bytes 1048576 | tf_op jit(solution)/shard_map/all_to_all | solution.py:61
  134.2 1.2 reshape.271
  135.5 1.3 fusion.11
  136.8 2.8 %convolution_convert_fusion.1 = bf16[256,1024]{1,0:T(8,128)(2,1)} fusion(bf16[256,1024]{1,0:T(8,128)(2,1)S(1)} %reshape.271, bf16[1,256,1024]{2,1,0:T(8,128)(2,1)} %param.43, bf16[1,1024,256]{2,1,0:T(8,128)(2,1)} %param.42, f32[256,256]{1,0:T(8,128)S(1)} %fusion.11), kind=kOutput, calls=%fused_computation.2 | convolution fusion | flops 269090816 | bytes 2359296 | tf_op jit(solution)/shard_map/dot_general | solution.py:122
  139.6 2.1 %reshape.272 = bf16[128,2,1024]{2,1,0:T(2,128)(2,1)} reshape(bf16[256,1024]{1,0:T(8,128)(2,1)} %convolution_convert_fusion.1) | data formatting | bytes 1048576 | tf_op jit(solution)/shard_map/reshape | solution.py:123
  141.7 10.1 %all-to-all-done.10 = bf16[64,4,1024]{2,1,0:T(4,128)(2,1)S(1)} async-done(((bf16[64,4,1024]{2,1,0:T(4,128)(2,1)}), bf16[64,4,1024]{2,1,0:T(4,128)(2,1)S(1)}, u32[]{:S(2)}, u32[]{:S(2)}) %all-to-all-start.10) | async-done | bytes 524320 | tf_op jit(solution)/shard_map/all_to_all | solution.py:61
  151.8 8.2 %all-to-all-start.6 = ((bf16[128,2,1024]{2,1,0:T(2,128)(2,1)}), bf16[128,2,1024]{2,1,0:T(2,128)(2,1)S(1)}, u32[]{:S(2)}, u32[]{:S(2)}) async-start(bf16[128,2,1024]{2,1,0:T(2,128)(2,1)} %reshape.272), calls=%async_computation.6 | async-start | bytes 1048576 | tf_op jit(solution)/shard_map/all_to_all | solution.py:233
  160.4 20.3 %all-to-all-done.6 = bf16[128,2,1024]{2,1,0:T(2,128)(2,1)S(1)} async-done(((bf16[128,2,1024]{2,1,0:T(2,128)(2,1)}), bf16[128,2,1024]{2,1,0:T(2,128)(2,1)S(1)}, u32[]{:S(2)}, u32[]{:S(2)}) %all-to-all-start.6) | async-done | bytes 524320 | tf_op jit(solution)/shard_map/all_to_all | solution.py:233
  (101 shorter events, 16.6 us)
Async XLA Ops:
  0.6 29.6 %copy-start = (bf16[4,1024,256]{2,1,0:T(8,128)(2,1)S(1)}, bf16[4,1024,256]{2,1,0:T(8,128)(2,1)}, u32[]{:S(2)}) copy-start(bf16[4,1024,256]{2,1,0:T(8,128)(2,1)} %param.26) | copy-start | bytes 6291460
  0.6 30.6 %copy-start.2 = (bf16[4,32,1024]{2,1,0:T(8,128)(2,1)S(1)}, bf16[4,32,1024]{2,1,0:T(8,128)(2,1)}, u32[]{:S(2)}) copy-start(bf16[4,32,1024]{2,1,0:T(8,128)(2,1)} %param.27) | copy-start | bytes 786436
  3.0 9.1 %all-to-all-start = ((bf16[4,4,1024]{2,1,0:T(4,128)(2,1)}), bf16[4,4,1024]{2,1,0:T(4,128)(2,1)S(1)}, u32[]{:S(2)}, u32[]{:S(2)}) async-start(bf16[4,4,1024]{2,1,0:T(4,128)(2,1)} %broadcast_in_dim.17), calls=%async_computation | async-start | bytes 65536 | tf_op jit(solution)/shard_map/all_to_all | solution.py:18
  15.3 7.4 %all-to-all-start.2 = ((f32[4,1,256]{2,1,0:T(1,128)}), f32[4,1,256]{2,1,0:T(1,128)S(1)}, u32[]{:S(2)}, u32[]{:S(2)}) async-start(f32[4,1,256]{2,1,0:T(1,128)} %reshape.286), calls=%async_computation.2 | async-start | bytes 8192 | tf_op jit(solution)/shard_map/all_to_all | solution.py:184
  22.7 7.5 %all-to-all-start.1 = ((bf16[16,2,288]{2,1,0:T(2,128)(2,1)}), bf16[16,2,288]{2,1,0:T(2,128)(2,1)S(1)}, u32[]{:S(2)}, u32[]{:S(2)}) async-start(bf16[16,2,288]{2,1,0:T(2,128)(2,1)} %copy.72), calls=%async_computation.1 | async-start | bytes 49152 | tf_op jit(solution)/shard_map/all_to_all | solution.py:35
  30.9 8.2 %copy-start.7 = (bf16[2,256,64]{1,2,0:T(8,128)(2,1)S(1)}, bf16[2,256,64]{1,2,0:T(8,128)(2,1)}, u32[]{:S(2)}) copy-start(bf16[2,256,64]{1,2,0:T(8,128)(2,1)} %param.37) | copy-start | bytes 196612
  30.9 8.4 %copy-start.1 = (bf16[128,1024]{1,0:T(8,128)(2,1)S(1)}, bf16[128,1024]{1,0:T(8,128)(2,1)}, u32[]{:S(2)}) copy-start(bf16[128,1024]{1,0:T(8,128)(2,1)} %param.38) | copy-start | bytes 786436
  30.9 15.4 %copy-start.3 = (bf16[4,1024]{1,0:T(4,128)(2,1)S(1)}, bf16[4,1024]{1,0:T(4,128)(2,1)}, u32[]{:S(2)}) copy-start(bf16[4,1024]{1,0:T(4,128)(2,1)} %param.24) | copy-start | bytes 24580
  30.9 15.4 %copy-start.9 = (f32[1024]{0:T(1024)S(1)}, f32[1024]{0:T(1024)}, u32[]{:S(2)}) copy-start(f32[1024]{0:T(1024)} %param.30) | copy-start | bytes 12292
  30.9 15.6 %copy-start.10 = (f32[1024]{0:T(1024)S(1)}, f32[1024]{0:T(1024)}, u32[]{:S(2)}) copy-start(f32[1024]{0:T(1024)} %param.47) | copy-start | bytes 12292
  30.9 15.6 %copy-start.11 = (f32[1024]{0:T(1024)S(1)}, f32[1024]{0:T(1024)}, u32[]{:S(2)}) copy-start(f32[1024]{0:T(1024)} %param.31) | copy-start | bytes 12292
  31.8 32.2 %copy-start.8 = (s32[4,6]{1,0:T(4,128)S(1)}, s32[4,6]{1,0:T(4,128)}, u32[]{:S(2)}) copy-start(s32[4,6]{1,0:T(4,128)} %param.39) | copy-start | bytes 292
  47.7 30.7 %all-to-all-start.7 = ((bf16[64,4,1024]{2,1,0:T(4,128)(2,1)}), bf16[64,4,1024]{2,1,0:T(4,128)(2,1)S(1)}, u32[]{:S(2)}, u32[]{:S(2)}) async-start(bf16[64,4,1024]{2,1,0:T(4,128)(2,1)} %broadcast_in_dim.24), calls=%async_computation.7 | async-start | bytes 1048576 | tf_op jit(solution)/shard_map/all_to_all | solution.py:18
  90.8 3.0 %copy-start.4 = (bf16[32,1024]{1,0:T(8,128)(2,1)S(1)}, bf16[32,1024]{1,0:T(8,128)(2,1)}, u32[]{:S(2)}) copy-start(bf16[32,1024]{1,0:T(8,128)(2,1)} %param.44) | copy-start | bytes 196612
  92.4 1.8 copy-start.5
  92.4 1.8 copy-start.6
  102.5 26.9 %all-to-all-start.5 = ((bf16[128,2,1024]{2,1,0:T(2,128)(2,1)}), bf16[128,2,1024]{2,1,0:T(2,128)(2,1)}, u32[]{:S(2)}, u32[]{:S(2)}) async-start(bf16[128,2,1024]{2,1,0:T(2,128)(2,1)} %reshape.270), calls=%async_computation.5 | async-start | bytes 1048576 | tf_op jit(solution)/shard_map/all_to_all | solution.py:231
  129.4 22.4 %all-to-all-start.10 = ((bf16[64,4,1024]{2,1,0:T(4,128)(2,1)}), bf16[64,4,1024]{2,1,0:T(4,128)(2,1)S(1)}, u32[]{:S(2)}, u32[]{:S(2)}) async-start(bf16[64,4,1024]{2,1,0:T(4,128)(2,1)} %reduce_sum.140), calls=%async_computation.10 | async-start | bytes 1048576 | tf_op jit(solution)/shard_map/all_to_all | solution.py:61
  139.6 41.9 %copy-start.13 = (f32[4,6]{1,0:T(4,128)S(1)}, f32[4,6]{1,0:T(4,128)}, u32[]{:S(2)}) copy-start(f32[4,6]{1,0:T(4,128)} %param.40) | copy-start | bytes 292
  139.6 42.2 %copy-start.12 = (f32[1024]{0:T(1024)S(1)}, f32[1024]{0:T(1024)}, u32[]{:S(2)}) copy-start(f32[1024]{0:T(1024)} %param.32) | copy-start | bytes 12292
  151.8 28.8 %all-to-all-start.6 = ((bf16[128,2,1024]{2,1,0:T(2,128)(2,1)}), bf16[128,2,1024]{2,1,0:T(2,128)(2,1)S(1)}, u32[]{:S(2)}, u32[]{:S(2)}) async-start(bf16[128,2,1024]{2,1,0:T(2,128)(2,1)} %reshape.272), calls=%async_computation.6 | async-start | bytes 1048576 | tf_op jit(solution)/shard_map/all_to_all | solution.py:233
where the time goes:
time: 184 us; the launch traced here: 182 us
  waiting for transfers between devices  66.3 us (36%)
  starting transfers between devices  47.3 us (26%)
  blocking collectives  30.1 us (16%)
  local copies, waits for them, and re-layouts  14.6 us (8%)
  matrix products  12.9 us (7%)
  other arithmetic  10.3 us (6%)
    all_to_all x2, starting transfers between devices, copy_for_each(): return lax.all_to_all(copies, axis, split_axis=0, concat_axis=0, tiled=True)  21.1 us
    all_to_all x1, waiting for transfers between devices, shards(): lax.all_to_all(result, EP, split_axis=0, concat_axis=0, tiled=True)  20.3 us
    all_to_all x1, waiting for transfers between devices, shards(): lax.all_to_all(outgoing, EP, split_axis=0, concat_axis=0, tiled=True)  18.4 us
    all_to_all x2, waiting for transfers between devices, copy_for_each(): return lax.all_to_all(copies, axis, split_axis=0, concat_axis=0, tiled=True)  13.5 us
    all_to_all x1, blocking collectives, copy_for_each(): return lax.all_to_all(copies, axis, split_axis=0, concat_axis=0, tiled=True)  12.1 us
    all_to_all x2, blocking collectives, sent_and_summed(): lax.all_to_all(parts, axis, split_axis=0, concat_axis=0, tiled=True)  11.2 us
    all_to_all x1, waiting for transfers between devices, summed_rows(): lax.all_to_all(own.astype(jnp.bfloat16), far, 0, 0, tiled=True)  10.1 us
    all_to_all x1, starting transfers between devices, shards(): lax.all_to_all(result, EP, split_axis=0, concat_axis=0, tiled=True)  8.24 us
  transfers between devices with their start and end apart: 7, of which 7 were waited for; matrix products, arithmetic and copies ran while one was open for 10% of the time, Pallas kernels for 0%

commit v1 on v0

v1 whole, which is shorter than its diff:
```python
import functools

import jax
import jax.numpy as jnp
from jax import lax
from jax.experimental import pallas as pl
from jax.experimental.pallas import tpu as pltpu
from jax.sharding import Mesh
from jax.sharding import PartitionSpec as P

EP = ("ep_0", "ep_1", "ep_2")
EP_TP = ("ep_0", "ep_1", "ep_2", "tp")
MESH = pl.DeviceIdType.MESH
F32 = jnp.float32
BF16 = jnp.bfloat16

epsilon = 1e-06
rope_base = 10000.0
negative = -1e30


def dot(a, b):
    return jnp.dot(a, b, preferred_element_type=F32)


def dot_nt(a, b):
    return lax.dot_general(a, b, (((1,), (1,)), ((), ())), preferred_element_type=F32)


def normalize(values, gain):
    values = values.astype(F32)
    mean = jnp.mean(values * values, axis=-1, keepdims=True)
    return values * lax.rsqrt(mean + epsilon) * gain


def swap_halves(values):
    half = values.shape[-1] // 2
    return jnp.concatenate([values[:, half:], values[:, :half]], axis=1)


def silu(values):
    return values / (1.0 + jnp.exp(-values))


def exchange(axis, size, me, src_of, dst, send, recv):
    copies = []
    for k in range(1, size):
        partner = lax.rem(me + k, size)
        copy = pltpu.make_async_remote_copy(
            src_ref=src_of(partner),
            dst_ref=dst.at[me],
            send_sem=send.at[k - 1],
            recv_sem=recv.at[me],
            device_id={axis: partner},
            device_id_type=MESH,
        )
        copy.start()
        copies.append(copy)
    return copies


def arrived(axis, size, me, dst, send, recv):
    for k in range(1, size):
        partner = lax.rem(me + k, size)
        pltpu.make_async_remote_copy(
            src_ref=dst.at[partner],
            dst_ref=dst.at[partner],
            send_sem=send.at[k - 1],
            recv_sem=recv.at[partner],
            device_id={axis: partner},
            device_id_type=MESH,
        ).wait_recv()


def greet(axes):
    barrier = pltpu.get_barrier_semaphore()
    total = 0
    for axis, size in axes:
        me = lax.axis_index(axis)
        for k in range(1, size):
            pl.semaphore_signal(
                barrier,
                inc=1,
                device_id={axis: lax.rem(me + k, size)},
                device_id_type=MESH,
            )
            total += 1
    pl.semaphore_wait(barrier, total)


def attention_kernel(
    sizes,
    lengths, tokens, cosines, sines, attn_gain, latent_gain, post_gain, ffn_gain,
    w_latent, w_rope_key, w_query, w_absorb_key, w_absorb_value, w_out,
    cache_latent, cache_rope,
    residual_out, ffn_out, latent_out, rope_out,
    lat, rop, hid, stack, qmsg_src, qmsg, fmsg_src, fmsg, wk_pad, q_lat, q_rot,
    att_src_f, att_src, att, att_stack, mix_src, mix,
    cache_sem, hid_send, hid_recv, q_send, q_recv, f_send, f_recv,
    att_send, att_recv, mix_send, mix_recv,
):
    nx = sizes["tp"]
    rows = tokens.shape[0]
    x = lax.axis_index("tp")
    lat_copy = pltpu.make_async_copy(cache_latent, lat, cache_sem.at[0])
    rop_copy = pltpu.make_async_copy(cache_rope, rop, cache_sem.at[1])
    lat_copy.start()
    rop_copy.start()
    greet((("tp", nx),))

    toks = tokens[...].astype(F32)
    hidden = normalize(toks, attn_gain[...]).astype(BF16)
    hid[x] = hidden
    hid_copies = exchange("tp", nx, x, lambda p: hid.at[x], hid, hid_send, hid_recv)
    cos = cosines[...]
    sin = sines[...]
    rope_pre = dot(hidden, w_rope_key[...])
    new_rope = (rope_pre * cos + swap_halves(rope_pre) * sin).astype(BF16)
    rope_out[...] = new_rope
    heads = w_absorb_key.shape[0]
    nope = w_absorb_key.shape[1]
    rank = w_absorb_key.shape[2]
    span = w_query.shape[1] // heads
    rope = span - nope
    wk_pad[...] = jnp.zeros(wk_pad.shape, BF16)
    for h in range(heads):
        wk_pad[h * span : h * span + nope, h * rank : (h + 1) * rank] = w_absorb_key[h]
    arrived("tp", nx, x, hid, hid_send, hid_recv)
    for t in range(nx):
        stack[t * rows : (t + 1) * rows, :] = hid[t].astype(F32)
    group_hidden = stack[...].astype(BF16)
    latent_part = dot(group_hidden, w_latent[...])
    queries = dot(group_hidden, w_query[...]).astype(BF16)
    query_latent = dot(queries, wk_pad[...])
    queries_f = queries.astype(F32)
    floats = jnp.concatenate(
        [latent_part] + [queries_f[:, h * span + nope : (h + 1) * span] for h in range(heads)],
        axis=1,
    )
    for t in range(nx):
        qmsg_src[t] = query_latent[t * rows : (t + 1) * rows, :].astype(BF16)
        fmsg_src[t] = floats[t * rows : (t + 1) * rows, :]
    qmsg[x] = qmsg_src[x]
    fmsg[x] = fmsg_src[x]
    q_copies = exchange("tp", nx, x, lambda p: qmsg_src.at[p], qmsg, q_send, q_recv)
    f_copies = exchange("tp", nx, x, lambda p: fmsg_src.at[p], fmsg, f_send, f_recv)
    arrived("tp", nx, x, fmsg, f_send, f_recv)
    part = w_latent.shape[1]
    pieces = [fmsg[t] for t in range(nx)]
    latent_full = jnp.concatenate([p[:, :part] for p in pieces], axis=1)
    new_latent = normalize(latent_full, latent_gain[...]).astype(BF16)
    latent_out[...] = new_latent
    for t in range(nx):
        for h in range(heads):
            for s in range(rows):
                n = t * heads + h
                q_rot[s, n : n + 1, :] = pieces[t][
                    s : s + 1, part + h * rope : part + (h + 1) * rope
                ]
    arrived("tp", nx, x, qmsg, q_send, q_recv)
    for t in range(nx):
        values = qmsg[t].astype(F32)
        for h in range(heads):
            for s in range(rows):
                n = t * heads + h
                q_lat[s, n : n + 1, :] = values[s : s + 1, h * rank : (h + 1) * rank]
    lat_copy.wait()
    rop_copy.wait()
    scaling = float(span) ** (-0.5)
    cached = lat.shape[1]
    position = lax.broadcasted_iota(jnp.int32, (nx * heads, cached), 1)
    latent_f = new_latent.astype(F32)
    rope_f = new_rope.astype(F32)
    for s in range(rows):
        ql_f = q_lat[s]
        ql = ql_f.astype(BF16)
        raw = q_rot[s]
        qr = (raw * cos[s : s + 1, :] + swap_halves(raw) * sin[s : s + 1, :]).astype(BF16)
        scores = (dot_nt(ql, lat[s]) + dot(qr, rop[s])) * scaling
        own = jnp.sum(ql_f * latent_f[s : s + 1, :], axis=-1, keepdims=True)
        own = (
            own + jnp.sum(qr.astype(F32) * rope_f[s : s + 1, :], axis=-1, keepdims=True)
        ) * scaling
        scores = jnp.where(position < lengths[s], scores, negative)
        top = jnp.maximum(jnp.max(scores, axis=-1, keepdims=True), own)
        weights = jnp.exp(scores - top)
        own_weight = jnp.exp(own - top)
        total = jnp.sum(weights, axis=-1, keepdims=True) + own_weight
        probs = (weights / total).astype(BF16)
        own_prob = (own_weight / total).astype(BF16).astype(F32)
        got = dot(probs, lat[s]) + own_prob * latent_f[s : s + 1, :]
        for t in range(nx):
            for h in range(heads):
                n = t * heads + h
                att_src_f[t, s : s + 1, h * rank : (h + 1) * rank] = got[n : n + 1, :]
    for t in range(nx):
        att_src[t] = att_src_f[t].astype(BF16)
    att[x] = att_src[x]
    att_copies = exchange("tp", nx, x, lambda p: att_src.at[p], att, att_send, att_recv)
    arrived("tp", nx, x, att, att_send, att_recv)
    for t in range(nx):
        att_stack[t * rows : (t + 1) * rows, :] = att[t].astype(F32)
    attended = att_stack[...].astype(BF16)
    v_head = w_absorb_value.shape[2]
    mixed = jnp.zeros((nx * rows, w_out.shape[1]), F32)
    for h in range(heads):
        head_out = dot(attended[:, h * rank : (h + 1) * rank], w_absorb_value[h]).astype(BF16)
        mixed = mixed + dot(head_out, w_out[h * v_head : (h + 1) * v_head, :])
    for t in range(nx):
        mix_src[t] = mixed[t * rows : (t + 1) * rows, :].astype(BF16)
    mix[x] = mix_src[x]
    mix_copies = exchange("tp", nx, x, lambda p: mix_src.at[p], mix, mix_send, mix_recv)
    arrived("tp", nx, x, mix, mix_send, mix_recv)
    total = mix[0].astype(F32)
    for t in range(1, nx):
        total = total + mix[t].astype(F32)
    residual = (toks + normalize(total, post_gain[...])).astype(BF16)
    residual_out[...] = residual
    ffn_out[...] = normalize(residual, ffn_gain[...]).astype(BF16)
    for copy in hid_copies + q_copies + f_copies + att_copies + mix_copies:
        copy.wait_send()


def expert_kernel(
    sizes,
    ffn_in, residual, routes, route_weights, out_gain, gate_vector,
    w_exp_gate, w_exp_up, w_exp_down, w_dense_gate, w_dense_up, w_dense_down,
    output,
    wg, wu, wd, dg, du, dd, gat0, gat1, stack0, stack1, x0, x1,
    o0, o1, r0, r1, t0, t1, s0, s1,
    w_sem, w_send, w_recv,
    g0_send, g0_recv, g1_send, g1_recv, x0_send, x0_recv, x1_send, x1_recv,
    r0_send, r0_recv, r1_send, r1_recv, s0_send, s0_recv, s1_send, s1_recv,
):
    nz, ny, nc = sizes["ep_0"], sizes["ep_1"], sizes["ep_2"]
    z, y, core = lax.axis_index("ep_0"), lax.axis_index("ep_1"), lax.axis_index("ep_2")
    rows, width = ffn_in.shape
    half = width // 2
    experts = nz * ny * nc
    pairs = (
        (w_exp_gate, wg), (w_exp_up, wu), (w_exp_down, wd),
        (w_dense_gate, dg), (w_dense_up, du), (w_dense_down, dd),
    )
    own_copies = [
        pltpu.make_async_copy(src, dst.at[core], w_sem.at[i])
        for i, (src, dst) in enumerate(pairs)
    ]
    for copy in own_copies:
        copy.start()
    greet((("ep_0", nz), ("ep_1", ny), ("ep_2", nc)))
    other = lax.rem(core + 1, nc)
    far_copies = [
        pltpu.make_async_remote_copy(
            src_ref=src, dst_ref=dst.at[core], send_sem=w_send.at[i], recv_sem=w_recv.at[i],
            device_id={"ep_2": other}, device_id_type=MESH,
        )
        for i, (src, dst) in enumerate(pairs)
    ]
    lane = lax.broadcasted_iota(jnp.int32, (rows, experts), 1)
    chosen = routes[...]
    given = route_weights[...]
    spread = jnp.zeros((rows, experts), F32)
    for k in range(routes.shape[1]):
        spread = spread + jnp.where(lane == chosen[:, k : k + 1], given[:, k : k + 1], 0.0)
    high = spread.astype(BF16)
    low = (spread - high.astype(F32)).astype(BF16)
    gat0[y] = jnp.concatenate([ffn_in[:, :half], high], axis=1)
    gat1[z] = jnp.concatenate([ffn_in[:, half:], low], axis=1)
    copies = exchange("ep_1", ny, y, lambda p: gat0.at[y], gat0, g0_send, g0_recv)
    copies += exchange("ep_0", nz, z, lambda p: gat1.at[z], gat1, g1_send, g1_recv)
    for copy in far_copies:
        copy.start()
    arrived("ep_1", ny, y, gat0, g0_send, g0_recv)
    for i in range(ny):
        stack0[i * rows : (i + 1) * rows, :] = gat0[i].astype(F32)
    x0[z] = stack0[...].astype(BF16)
    copies += exchange("ep_0", nz, z, lambda p: x0.at[z], x0, x0_send, x0_recv)
    arrived("ep_0", nz, z, gat1, g1_send, g1_recv)
    for i in range(nz):
        stack1[i * rows : (i + 1) * rows, :] = gat1[i].astype(F32)
    x1[y] = stack1[...].astype(BF16)
    copies += exchange("ep_1", ny, y, lambda p: x1.at[y], x1, x1_send, x1_recv)
    count = nz * ny * rows
    to = lax.broadcasted_iota(jnp.int32, (count, count), 0)
    fro = lax.broadcasted_iota(jnp.int32, (count, count), 1)
    to_z, to_y, to_r = to // (ny * rows), (to // rows) % ny, to % rows
    swap = jnp.where(fro == to_y * (nz * rows) + to_z * rows + to_r, 1.0, 0.0).astype(BF16)
    swap_back = jnp.where(to == (fro // rows) % ny * (nz * rows) + fro // (ny * rows) * rows + fro % rows, 1.0, 0.0).astype(BF16)
    for copy in own_copies:
        copy.wait()
    for copy in far_copies:
        copy.wait()
    arrived("ep_0", nz, z, x0, x0_send, x0_recv)
    arrived("ep_1", ny, y, x1, x1_send, x1_recv)
    first = x0[...].reshape(count, half + experts)
    second = dot(swap, x1[...].reshape(count, half + experts)).astype(BF16)
    every = jnp.concatenate([first[:, :half], second[:, :half]], axis=1)
    spread = first[:, half:].astype(F32) + second[:, half:].astype(F32)
    columns = lax.broadcasted_iota(jnp.int32, (count, experts), 1)
    chip = (z * ny + y) * nc
    acts = []
    for e in range(nc):
        weight = jnp.sum(jnp.where(columns == chip + e, spread, 0.0), axis=1, keepdims=True)
        act = silu(dot(every, wg[e, 0])) * dot(every, wu[e, 0])
        acts.append((act * weight).astype(BF16))
    acts = jnp.concatenate(acts, axis=1)
    gate = jnp.sum(every.astype(F32) * gate_vector[...], axis=1, keepdims=True)
    gate = 1.0 / (1.0 + jnp.exp(-gate))
    units = nc * dg.shape[1]
    dense = silu(dot_nt(every, dg[...].reshape(units, width))) * dot_nt(
        every, du[...].reshape(units, width)
    )
    dense = (dense * gate).astype(BF16)
    down = wd[...].reshape(nc * wd.shape[2], width)
    dense_down = dd[...].reshape(units, width)
    part0 = dot(acts, down[:, :half]) + dot(dense, dense_down[:, :half])
    o0[...] = part0.astype(BF16).reshape(o0.shape)
    copies += exchange("ep_0", nz, z, lambda p: o0.at[p], r0, r0_send, r0_recv)
    acts_swapped = dot(swap_back, acts).astype(BF16)
    dense_swapped = dot(swap_back, dense).astype(BF16)
    part1 = dot(acts_swapped, down[:, half:]) + dot(dense_swapped, dense_down[:, half:])
    o1[...] = part1.astype(BF16).reshape(o1.shape)
    copies += exchange("ep_1", ny, y, lambda p: o1.at[p], r1, r1_send, r1_recv)
    r0[z] = o0[z]
    r1[y] = o1[y]
    arrived("ep_0", nz, z, r0, r0_send, r0_recv)
    total = r0[0].astype(F32)
    for i in range(1, nz):
        total = total + r0[i].astype(F32)
    for i in range(ny):
        t0[i] = total[i * rows : (i + 1) * rows, :].astype(BF16)
    copies += exchange("ep_1", ny, y, lambda p: t0.at[p], s0, s0_send, s0_recv)
    arrived("ep_1", ny, y, r1, r1_send, r1_recv)
    total = r1[0].astype(F32)
    for i in range(1, ny):
        total = total + r1[i].astype(F32)
    for i in range(nz):
        t1[i] = total[i * rows : (i + 1) * rows, :].astype(BF16)
    copies += exchange("ep_0", nz, z, lambda p: t1.at[p], s1, s1_send, s1_recv)
    s0[y] = t0[y]
    s1[z] = t1[z]
    arrived("ep_1", ny, y, s0, s0_send, s0_recv)
    arrived("ep_0", nz, z, s1, s1_send, s1_recv)
    left = s0[0].astype(F32)
    for i in range(1, ny):
        left = left + s0[i].astype(F32)
    right = s1[0].astype(F32)
    for i in range(1, nz):
        right = right + s1[i].astype(F32)
    combined = jnp.concatenate([left, right], axis=1)
    output[...] = (residual[...].astype(F32) + normalize(combined, out_gain[...])).astype(BF16)
    for copy in copies:
        copy.wait_send()


def in_vmem(count):
    return [pl.BlockSpec(memory_space=pltpu.VMEM)] * count


def in_place(count):
    return [pl.BlockSpec(memory_space=pl.ANY)] * count


def semaphores(*counts):
    return [pltpu.SemaphoreType.DMA((n,)) for n in counts]


def shards(
    sizes,
    tokens,
    lengths,
    cache_latent,
    cache_rope,
    attn_gain,
    latent_gain,
    post_gain,
    ffn_gain,
    out_gain,
    w_latent,
    w_rope_key,
    w_query,
    w_absorb_key,
    w_absorb_value,
    w_out,
    routes,
    route_weights,
    w_exp_gate,
    w_exp_up,
    w_exp_down,
    w_dense_gate,
    w_dense_up,
    w_dense_down,
    dense_gate_vector,
):
    rows, width = tokens.shape
    nz, ny, nc, nx = sizes["ep_0"], sizes["ep_1"], sizes["ep_2"], sizes["tp"]
    half = width // 2
    experts = nz * ny * nc
    heads, nope, rank = w_absorb_key.shape
    rope = w_rope_key.shape[1]
    part = w_latent.shape[1]
    floats = part + heads * rope
    inverse = rope_base ** (-jnp.arange(rope // 2, dtype=F32) / (rope // 2))
    angles = lengths.astype(F32)[:, None] * inverse
    cosines = jnp.concatenate([jnp.cos(angles)] * 2, axis=1)
    sine = jnp.sin(angles)
    sines = jnp.concatenate([-sine, sine], axis=1)
    V = pltpu.VMEM
    residual, ffn_in, new_latent, new_rope = pl.pallas_call(
        functools.partial(attention_kernel, sizes),
        out_shape=(
            jax.ShapeDtypeStruct((rows, width), BF16),
            jax.ShapeDtypeStruct((rows, width), BF16),
            jax.ShapeDtypeStruct((rows, rank), BF16),
            jax.ShapeDtypeStruct((rows, rope), BF16),
        ),
        in_specs=[pl.BlockSpec(memory_space=pltpu.SMEM)] + in_vmem(13) + in_place(2),
        out_specs=tuple(in_vmem(4)),
        scratch_shapes=[
            V(cache_latent.shape, BF16),
            V(cache_rope.shape, BF16),
            V((nx, rows, width), BF16),
            V((nx * rows, width), F32),
            V((nx, rows, heads * rank), BF16),
            V((nx, rows, heads * rank), BF16),
            V((nx, rows, floats), F32),
            V((nx, rows, floats), F32),
            V((w_query.shape[1], heads * rank), BF16),
            V((rows, nx * heads, rank), F32),
            V((rows, nx * heads, rope), F32),
            V((nx, rows, heads * rank), F32),
            V((nx, rows, heads * rank), BF16),
            V((nx, rows, heads * rank), BF16),
            V((nx * rows, heads * rank), F32),
            V((nx, rows, width), BF16),
            V((nx, rows, width), BF16),
        ]
        + semaphores(2, *([nx - 1, nx] * 5)),
        compiler_params=pltpu.CompilerParams(collective_id=0, has_side_effects=True),
        cost_estimate=pl.CostEstimate(flops=10**8, bytes_accessed=4 * 10**6, transcendentals=0),
        name="attention",
    )(
        lengths, tokens, cosines, sines, attn_gain[None], latent_gain[None], post_gain[None],
        ffn_gain[None], w_latent, w_rope_key, w_query, w_absorb_key, w_absorb_value, w_out,
        cache_latent, cache_rope,
    )
    output = pl.pallas_call(
        functools.partial(expert_kernel, sizes),
        out_shape=jax.ShapeDtypeStruct((rows, width), BF16),
        in_specs=in_vmem(6) + in_place(6),
        out_specs=in_vmem(1)[0],
        scratch_shapes=[
            V((nc, *w_exp_gate.shape), BF16),
            V((nc, *w_exp_up.shape), BF16),
            V((nc, *w_exp_down.shape), BF16),
            V((nc, *w_dense_gate.shape), BF16),
            V((nc, *w_dense_up.shape), BF16),
            V((nc, *w_dense_down.shape), BF16),
            V((ny, rows, half + experts), BF16),
            V((nz, rows, half + experts), BF16),
            V((ny * rows, half + experts), F32),
            V((nz * rows, half + experts), F32),
            V((nz, ny * rows, half + experts), BF16),
            V((ny, nz * rows, half + experts), BF16),
            V((nz, ny * rows, half), BF16),
            V((ny, nz * rows, half), BF16),
            V((nz, ny * rows, half), BF16),
            V((ny, nz * rows, half), BF16),
            V((ny, rows, half), BF16),
            V((nz, rows, half), BF16),
            V((ny, rows, half), BF16),
            V((nz, rows, half), BF16),
        ]
        + semaphores(6, 6, 6, *([ny - 1, ny, nz - 1, nz, nz - 1, nz, ny - 1, ny] * 2)),
        compiler_params=pltpu.CompilerParams(collective_id=1, has_side_effects=True),
        cost_estimate=pl.CostEstimate(flops=10**9, bytes_accessed=4 * 10**6, transcendentals=0),
        name="experts",
    )(
        ffn_in, residual, routes, route_weights, out_gain[None], dense_gate_vector[None],
        w_exp_gate, w_exp_up, w_exp_down, w_dense_gate, w_dense_up, w_dense_down,
    )
    return (output, new_latent, new_rope)


def solution(mesh, dims=(8, 8, 2)):
    torus = Mesh(mesh.devices.reshape(*dims, mesh.shape["tp"]), EP_TP)
    placed = (
        P(EP_TP, None),
        P(EP_TP),
        P(EP_TP, None, None),
        P(EP_TP, None, None),
        P(),
        P(),
        P(),
        P(),
        P(),
        P(None, "tp"),
        P(),
        P(None, "tp"),
        P("tp", None, None),
        P("tp", None, None),
        P("tp", None),
        P(EP_TP, None),
        P(EP_TP, None),
        P(EP, None, None),
        P(EP, None, None),
        P(EP, None, None),
        P(EP, None),
        P(EP, None),
        P(EP, None),
        P(),
    )
    return jax.shard_map(
        functools.partial(shards, dict(torus.shape)),
        mesh=torus,
        in_specs=placed,
        out_specs=(P(EP_TP, None), P(EP_TP, None), P(EP_TP, None)),
        check_vma=False,
    )
```

time: 184 us -> 78.5 us (0.43)
  the two profiles are of different devices: /device:TPU:1 before, /device:TPU:16 now
where the time goes in v1:
time: 78.5 us; the launch traced here: 78 us
  Pallas kernels  66.5 us (85%)
  local copies, waits for them, and re-layouts  9.45 us (12%)
  other arithmetic  1.44 us (2%)
    pallas_call x1, Pallas kernels, shards(): pl.pallas_call(functools.partial(expert_kernel, sizes), out_shape=jax.Sha...  42.4 us
    pallas_call x1, Pallas kernels, shards(): pl.pallas_call(functools.partial(attention_kernel, sizes), out_shape=(jax...  24.1 us
    unnamed x11, local copies, waits for them, and re-layouts  9.45 us

profile of v1, /device:TPU:16, one launch (start us, length us, event | category | flops | bytes accessed | tf_op | source)
XLA Modules:
  0.0 78.0 jit_solution(15653887579566275948)
XLA Ops:
  0.6 0.7 convert_element_type.3
  1.3 0.1 fusion
  1.4 0.7 pad_maximum_fusion
  2.1 1.6 %copy.30.w_absorb_value = bf16[2,256,64]{2,1,0:T(8,128)(2,1)} copy(bf16[2,256,64]{1,2,0:T(8,128)(2,1)} %param.37) | data formatting | bytes 131072 | tf_op args[13]
  3.7 1.7 %copy.27.w_latent = bf16[1024,64]{1,0:T(8,128)(2,1)} copy(bf16[1024,64]{0,1:T(8,128)(2,1)} %param.33) | data formatting | bytes 262144 | tf_op args[9]
  5.4 1.7 %copy.28.w_rope_key = bf16[1024,32]{1,0:T(8,128)(2,1)} copy(bf16[1024,32]{0,1:T(8,128)(2,1)} %param.34) | data formatting | bytes 131072 | tf_op args[10]
  7.1 2.0 %copy.29.w_query = bf16[1024,192]{1,0:T(8,128)(2,1)} copy(bf16[1024,192]{0,1:T(8,128)(2,1)} %param.35) | data formatting | bytes 786432 | tf_op args[11]
  9.1 24.1 %attention.1 = (bf16[4,1024]{1,0:T(4,128)(2,1)}, bf16[4,1024]{1,0:T(4,128)(2,1)}, bf16[4,256]{1,0:T(4,128)(2,1)}, bf16[4,32]{1,0:T(4,128)(2,1)}) custom-call(s32[4]{0:T(128)} %lengths.1, bf16[4,1024]{1,0:T(4,128)(2,1)} %tokens.1, f32[4,32]{1,0:T(4,128)} %get-tuple-element.14.cosines, f32[4,32]{1,0:T(4,128)} %get-tuple-element.15.sines, f32[1,1024]{1,0:T(1,128)} %bitcast.6, ...), custom_call_target="tpu_custom_call" | custom-call | flops 100000000 | bytes 4000000 | tf_op jit(solution)/shard_map/attention/pallas_call | solution.py:409
  33.2 0.0 copy-start
  33.2 0.0 copy-start.1
  33.2 42.4 %experts.1 = bf16[4,1024]{1,0:T(4,128)(2,1)} custom-call(bf16[4,1024]{1,0:T(4,128)(2,1)} %get-tuple-element.7.ffn_in, bf16[4,1024]{1,0:T(4,128)(2,1)} %get-tuple-element.8.residual, s32[4,6]{1,0:T(4,128)} %routes.1, f32[4,6]{1,0:T(4,128)} %route_weights.1, f32[1,1024]{1,0:T(1,128)} %bitcast.10, f32[1,1024]{1,0:T(1,128)} %bitcast.11, ...), custom_call_target="tpu_custom_call" | custom-call | flops 1000000000 | bytes 4000000 | tf_op jit(solution)/shard_map/experts/pallas_call | solution.py:447
  75.6 1.3 %copy.34 = bf16[4,1024]{1,0:T(4,128)(2,1)} copy(bf16[4,1024]{1,0:T(4,128)(2,1)} %experts.1) | data formatting | bytes 16384
  76.9 0.0 copy-done
  76.9 0.6 copy.35
  77.5 0.0 copy-done.1
  77.5 0.6 copy.36
  (1 shorter events, 0.0 us)
Async XLA Ops:
  33.2 43.7 %copy-start = (bf16[4,256]{1,0:T(4,128)(2,1)S(1)}, bf16[4,256]{1,0:T(4,128)(2,1)}, u32[]{:S(2)}) copy-start(bf16[4,256]{1,0:T(4,128)(2,1)} %get-tuple-element.20) | copy-start | bytes 6148
  33.2 44.3 %copy-start.1 = (bf16[4,32]{1,0:T(4,128)(2,1)S(1)}, bf16[4,32]{1,0:T(4,128)(2,1)}, u32[]{:S(2)}) copy-start(bf16[4,32]{1,0:T(4,128)(2,1)} %get-tuple-element.21) | copy-start | bytes 772

commit v2 on v1

v2 whole, which is shorter than its diff:
```python
import functools

import jax
import jax.numpy as jnp
import numpy as np
from jax import lax
from jax.experimental import pallas as pl
from jax.experimental.pallas import tpu as pltpu
from jax.sharding import Mesh
from jax.sharding import PartitionSpec as P

EP = ("ep_0", "ep_1", "ep_2")
EP_TP = ("ep_0", "ep_1", "ep_2", "tp")
MESH = pl.DeviceIdType.MESH
F32 = jnp.float32
BF16 = jnp.bfloat16

epsilon = 1e-06
rope_base = 10000.0
negative = -1e30


def dot(a, b):
    return jnp.dot(a, b, preferred_element_type=F32)


def dot_nt(a, b):
    return lax.dot_general(a, b, (((1,), (1,)), ((), ())), preferred_element_type=F32)


def normalize(values, gain):
    values = values.astype(F32)
    mean = jnp.mean(values * values, axis=-1, keepdims=True)
    return values * lax.rsqrt(mean + epsilon) * gain


def swap_halves(values):
    half = values.shape[-1] // 2
    return jnp.concatenate([values[:, half:], values[:, :half]], axis=1)


def silu(values):
    return values / (1.0 + jnp.exp(-values))


def exchange(axis, size, me, src_of, dst, send, recv):
    copies = []
    for k in range(1, size):
        partner = lax.rem(me + k, size)
        copy = pltpu.make_async_remote_copy(
            src_ref=src_of(partner),
            dst_ref=dst.at[me],
            send_sem=send.at[k - 1],
            recv_sem=recv.at[me],
            device_id={axis: partner},
            device_id_type=MESH,
        )
        copy.start()
        copies.append(copy)
    return copies


def arrived(axis, size, me, dst, send, recv):
    for k in range(1, size):
        partner = lax.rem(me + k, size)
        pltpu.make_async_remote_copy(
            src_ref=dst.at[partner],
            dst_ref=dst.at[partner],
            send_sem=send.at[k - 1],
            recv_sem=recv.at[partner],
            device_id={axis: partner},
            device_id_type=MESH,
        ).wait_recv()


def greet(axes):
    barrier = pltpu.get_barrier_semaphore()
    total = 0
    for axis, size in axes:
        me = lax.axis_index(axis)
        for k in range(1, size):
            pl.semaphore_signal(
                barrier,
                inc=1,
                device_id={axis: lax.rem(me + k, size)},
                device_id_type=MESH,
            )
            total += 1
    return barrier, total


def stack_rows(blocks, stack, count, rows):
    for i in range(count):
        stack[i * rows : (i + 1) * rows, :] = blocks[i].astype(F32)
    return stack[...].astype(BF16)


def added(blocks, count):
    total = blocks[0].astype(F32)
    for i in range(1, count):
        total = total + blocks[i].astype(F32)
    return total


def layer_kernel(
    sizes,
    stop,
    lengths, tokens_in, inverse_in, attn_gain_in, latent_gain_in, post_gain_in, ffn_gain_in,
    out_gain_in, gate_vector_in, routes_in, route_weights_in,
    w_latent, w_rope_key, w_query, w_absorb_key, w_absorb_value, w_out,
    cache_latent, cache_rope,
    w_exp_gate, w_exp_up, w_exp_down, w_dense_gate, w_dense_up, w_dense_down,
    output, latent_out, rope_out,
    tokens, inverse, attn_gain, latent_gain, post_gain, ffn_gain, out_gain, gate_vector,
    routes, route_weights, w_front, w_rope, wk, wv, wo, lat, rop, wg, wu, wd, dg, du, dd,
    hid, stack, qmsg_src, qmsg, fmsg_src, fmsg, wk_pad, q_lat, q_rot,
    att_src_f, att_src, att, att_stack, mix_src, mix,
    gw0, gw1, stack_w0, stack_w1, w0, w1, gat0, gat1, stack0, stack1, x0, x1,
    o0, o1, r0, r1, t0, t1, s0, s1,
    in_sem, far_send, far_recv,
    hid_send, hid_recv, q_send, q_recv, f_send, f_recv,
    att_send, att_recv, mix_send, mix_recv,
    gw0_send, gw0_recv, gw1_send, gw1_recv, w0_send, w0_recv, w1_send, w1_recv,
    g0_send, g0_recv, g1_send, g1_recv, x0_send, x0_recv, x1_send, x1_recv,
    r0_send, r0_recv, r1_send, r1_recv, s0_send, s0_recv, s1_send, s1_recv,
):
    nz, ny, nc, nx = sizes["ep_0"], sizes["ep_1"], sizes["ep_2"], sizes["tp"]
    z, y, core = lax.axis_index("ep_0"), lax.axis_index("ep_1"), lax.axis_index("ep_2")
    x = lax.axis_index("tp")
    rows, width = tokens.shape
    half = width // 2
    experts = nz * ny * nc
    heads, nope, rank = w_absorb_key.shape
    part = w_latent.shape[0]
    rope = w_rope_key.shape[0]
    span = nope + rope
    barrier, total = greet((("tp", nx), ("ep_2", nc), ("ep_1", ny), ("ep_0", nz)))

    moves = [
        (tokens_in, tokens), (attn_gain_in, attn_gain),
        (routes_in, routes), (route_weights_in, route_weights), (inverse_in, inverse),
    ]
    front = [(w_rope_key, w_rope)]
    for h in range(heads):
        front.append((w_query.at[pl.ds(h * span, nope)], w_front.at[pl.ds(h * nope, nope)]))
    front.append((w_latent, w_front.at[pl.ds(heads * nope, part)]))
    for h in range(heads):
        front.append(
            (
                w_query.at[pl.ds(h * span + nope, rope)],
                w_front.at[pl.ds(heads * nope + part + h * rope, rope)],
            )
        )
    front.append((w_absorb_key, wk))
    middle = [
        (latent_gain_in, latent_gain), (cache_latent, lat), (cache_rope, rop),
        (w_absorb_value, wv), (w_out, wo), (post_gain_in, post_gain), (ffn_gain_in, ffn_gain),
        (out_gain_in, out_gain), (gate_vector_in, gate_vector),
    ]
    pairs = [
        (w_exp_gate, wg), (w_exp_up, wu), (w_exp_down, wd),
        (w_dense_gate, dg), (w_dense_up, du), (w_dense_down, dd),
    ]
    back = [(src, dst.at[core]) for src, dst in pairs]
    started = []
    for src, dst in moves + front + middle + back:
        copy = pltpu.make_async_copy(src, dst, in_sem.at[len(started)])
        copy.start()
        started.append(copy)
    waiting = iter(started)

    def take(count):
        for _ in range(count):
            next(waiting).wait()

    take(len(moves))
    toks = tokens[...].astype(F32)
    hidden = normalize(toks, attn_gain[...]).astype(BF16)
    hid[x] = hidden
    lane = lax.broadcasted_iota(jnp.int32, (rows, experts), 1)
    chosen = routes[...]
    given = route_weights[...]
    spread = jnp.zeros((rows, experts), F32)
    for k in range(routes.shape[1]):
        spread = spread + jnp.where(lane == chosen[:, k : k + 1], given[:, k : k + 1], 0.0)
    high = spread.astype(BF16)
    gw0[y] = high
    gw1[z] = (spread - high.astype(F32)).astype(BF16)

    pl.semaphore_wait(barrier, total)
    sent = []

    def finish():
        for copy in waiting:
            copy.wait()
        for copy in sent:
            copy.wait_send()
        output[...] = toks.astype(BF16)

    sent += exchange("tp", nx, x, lambda p: hid.at[x], hid, hid_send, hid_recv)
    other = lax.rem(core + 1, nc)
    far = [
        pltpu.make_async_remote_copy(
            src_ref=src, dst_ref=dst.at[core], send_sem=far_send.at[i], recv_sem=far_recv.at[i],
            device_id={"ep_2": other}, device_id_type=MESH,
        )
        for i, (src, dst) in enumerate(pairs)
    ]
    for copy in far:
        copy.start()
    sent += exchange("ep_1", ny, y, lambda p: gw0.at[y], gw0, gw0_send, gw0_recv)
    sent += exchange("ep_0", nz, z, lambda p: gw1.at[z], gw1, gw1_send, gw1_recv)

    row = lax.broadcasted_iota(jnp.int32, (rows, rope), 0)
    held = jnp.zeros((rows, rope), F32)
    for s in range(rows):
        held = jnp.where(row == s, lengths[s].astype(F32), held)
    angles = held * inverse[...]
    cos = jnp.cos(angles)
    sin = jnp.sin(angles)
    first_half = lax.broadcasted_iota(jnp.int32, (rows, rope), 1) < rope // 2
    sin = jnp.where(first_half, -sin, sin)
    wk_pad[...] = jnp.zeros(wk_pad.shape, BF16)
    take(len(front))
    for h in range(heads):
        wk_pad[h * nope : (h + 1) * nope, h * rank : (h + 1) * rank] = wk[h]
    rope_pre = dot_nt(hidden, w_rope[...])
    new_rope = (rope_pre * cos + swap_halves(rope_pre) * sin).astype(BF16)
    rope_out[...] = new_rope
    arrived("tp", nx, x, hid, hid_send, hid_recv)
    if stop == 1:
        for copy in far:
            copy.wait()
        arrived("ep_1", ny, y, gw0, gw0_send, gw0_recv)
        arrived("ep_0", nz, z, gw1, gw1_send, gw1_recv)
        return finish()
    projected = dot_nt(stack_rows(hid, stack, nx, rows), w_front[...])
    flat = heads * nope
    query_latent = dot(projected[:, :flat].astype(BF16), wk_pad[...])
    for t in range(nx):
        qmsg_src[t] = query_latent[t * rows : (t + 1) * rows, :].astype(BF16)
        fmsg_src[t] = projected[t * rows : (t + 1) * rows, flat:]
    sent += exchange("tp", nx, x, lambda p: fmsg_src.at[p], fmsg, f_send, f_recv)
    sent += exchange("tp", nx, x, lambda p: qmsg_src.at[p], qmsg, q_send, q_recv)
    qmsg[x] = qmsg_src[x]
    fmsg[x] = fmsg_src[x]
    arrived("ep_1", ny, y, gw0, gw0_send, gw0_recv)
    arrived("ep_0", nz, z, gw1, gw1_send, gw1_recv)
    w0[z] = stack_rows(gw0, stack_w0, ny, rows)
    w1[y] = stack_rows(gw1, stack_w1, nz, rows)
    arrived("tp", nx, x, fmsg, f_send, f_recv)
    pieces = [fmsg[t] for t in range(nx)]
    latent_full = jnp.concatenate([p[:, :part] for p in pieces], axis=1)
    take(len(middle))
    new_latent = normalize(latent_full, latent_gain[...]).astype(BF16)
    latent_out[...] = new_latent
    for t in range(nx):
        values = pieces[t].astype(BF16).astype(F32)
        for h in range(heads):
            for s in range(rows):
                n = t * heads + h
                q_rot[s, n : n + 1, :] = values[
                    s : s + 1, part + h * rope : part + (h + 1) * rope
                ]
    arrived("tp", nx, x, qmsg, q_send, q_recv)
    sent += exchange("ep_0", nz, z, lambda p: w0.at[z], w0, w0_send, w0_recv)
    sent += exchange("ep_1", ny, y, lambda p: w1.at[y], w1, w1_send, w1_recv)
    for t in range(nx):
        values = qmsg[t].astype(F32)
        for h in range(heads):
            for s in range(rows):
                n = t * heads + h
                q_lat[s, n : n + 1, :] = values[s : s + 1, h * rank : (h + 1) * rank]

    def early():
        for copy in far:
            copy.wait()
        arrived("ep_0", nz, z, w0, w0_send, w0_recv)
        arrived("ep_1", ny, y, w1, w1_send, w1_recv)

    if stop == 2:
        early()
        return finish()
    scaling = float(span) ** (-0.5)
    cached = lat.shape[1]
    position = lax.broadcasted_iota(jnp.int32, (nx * heads, cached), 1)
    latent_f = new_latent.astype(F32)
    rope_f = new_rope.astype(F32)
    for s in range(rows):
        ql_f = q_lat[s]
        raw = q_rot[s]
        qr = (raw * cos[s : s + 1, :] + swap_halves(raw) * sin[s : s + 1, :]).astype(BF16)
        scores = (dot_nt(ql_f.astype(BF16), lat[s]) + dot(qr, rop[s])) * scaling
        own = jnp.sum(ql_f * latent_f[s : s + 1, :], axis=-1, keepdims=True)
        own = (
            own + jnp.sum(qr.astype(F32) * rope_f[s : s + 1, :], axis=-1, keepdims=True)
        ) * scaling
        scores = jnp.where(position < lengths[s], scores, negative)
        top = jnp.maximum(jnp.max(scores, axis=-1, keepdims=True), own)
        weights = jnp.exp(scores - top)
        own_weight = jnp.exp(own - top)
        whole = jnp.sum(weights, axis=-1, keepdims=True) + own_weight
        probs = (weights / whole).astype(BF16)
        own_prob = (own_weight / whole).astype(BF16).astype(F32)
        got = dot(probs, lat[s]) + own_prob * latent_f[s : s + 1, :]
        for t in range(nx):
            for h in range(heads):
                n = t * heads + h
                att_src_f[t, s : s + 1, h * rank : (h + 1) * rank] = got[n : n + 1, :]
    for t in range(nx):
        att_src[t] = att_src_f[t].astype(BF16)
    sent += exchange("tp", nx, x, lambda p: att_src.at[p], att, att_send, att_recv)
    att[x] = att_src[x]
    if stop == 3:
        arrived("tp", nx, x, att, att_send, att_recv)
        early()
        return finish()
    count = nz * ny * rows
    to = lax.broadcasted_iota(jnp.int32, (count, count), 0)
    fro = lax.broadcasted_iota(jnp.int32, (count, count), 1)
    source = to // rows % ny * (nz * rows) + to // (ny * rows) * rows + to % rows
    swap = jnp.where(fro == source, 1.0, 0.0).astype(BF16)
    source = fro // rows % ny * (nz * rows) + fro // (ny * rows) * rows + fro % rows
    swap_back = jnp.where(to == source, 1.0, 0.0).astype(BF16)
    early()
    spread = w0[...].reshape(count, experts).astype(F32) + dot(
        swap, w1[...].reshape(count, experts)
    )
    columns = lax.broadcasted_iota(jnp.int32, (count, experts), 1)
    chip = (z * ny + y) * nc
    shares = [
        jnp.sum(jnp.where(columns == chip + e, spread, 0.0), axis=1, keepdims=True)
        for e in range(nc)
    ]
    arrived("tp", nx, x, att, att_send, att_recv)
    attended = stack_rows(att, att_stack, nx, rows)
    v_head = wv.shape[1]
    mixed = jnp.zeros((nx * rows, width), F32)
    for h in range(heads):
        head_out = dot_nt(attended[:, h * rank : (h + 1) * rank], wv[h]).astype(BF16)
        mixed = mixed + dot(head_out, wo[h * v_head : (h + 1) * v_head, :])
    for t in range(nx):
        mix_src[t] = mixed[t * rows : (t + 1) * rows, :].astype(BF16)
    sent += exchange("tp", nx, x, lambda p: mix_src.at[p], mix, mix_send, mix_recv)
    mix[x] = mix_src[x]
    arrived("tp", nx, x, mix, mix_send, mix_recv)
    if stop == 4:
        return finish()
    residual = (toks + normalize(added(mix, nx), post_gain[...])).astype(BF16)
    ffn_in = normalize(residual, ffn_gain[...]).astype(BF16)

    gat0[y] = ffn_in[:, :half]
    gat1[z] = ffn_in[:, half:]
    sent += exchange("ep_1", ny, y, lambda p: gat0.at[y], gat0, g0_send, g0_recv)
    sent += exchange("ep_0", nz, z, lambda p: gat1.at[z], gat1, g1_send, g1_recv)
    arrived("ep_1", ny, y, gat0, g0_send, g0_recv)
    x0[z] = stack_rows(gat0, stack0, ny, rows)
    sent += exchange("ep_0", nz, z, lambda p: x0.at[z], x0, x0_send, x0_recv)
    arrived("ep_0", nz, z, gat1, g1_send, g1_recv)
    x1[y] = stack_rows(gat1, stack1, nz, rows)
    sent += exchange("ep_1", ny, y, lambda p: x1.at[y], x1, x1_send, x1_recv)
    if stop == 5:
        arrived("ep_0", nz, z, x0, x0_send, x0_recv)
        arrived("ep_1", ny, y, x1, x1_send, x1_recv)
        return finish()
    take(len(back))
    arrived("ep_0", nz, z, x0, x0_send, x0_recv)
    arrived("ep_1", ny, y, x1, x1_send, x1_recv)
    first = x0[...].reshape(count, half)
    second = dot(swap, x1[...].reshape(count, half)).astype(BF16)
    every = jnp.concatenate([first, second], axis=1)
    acts = []
    for e in range(nc):
        act = silu(dot(every, wg[e, 0])) * dot(every, wu[e, 0])
        acts.append((act * shares[e]).astype(BF16))
    acts = jnp.concatenate(acts, axis=1)
    gate = jnp.sum(every.astype(F32) * gate_vector[...], axis=1, keepdims=True)
    gate = 1.0 / (1.0 + jnp.exp(-gate))
    units = nc * dg.shape[1]
    dense = silu(dot_nt(every, dg[...].reshape(units, width))) * dot_nt(
        every, du[...].reshape(units, width)
    )
    dense = (dense * gate).astype(BF16)
    down = wd[...].reshape(nc * wd.shape[2], width)
    dense_down = dd[...].reshape(units, width)
    part0 = dot(acts, down[:, :half]) + dot(dense, dense_down[:, :half])
    o0[...] = part0.astype(BF16).reshape(o0.shape)
    sent += exchange("ep_0", nz, z, lambda p: o0.at[p], r0, r0_send, r0_recv)
    acts_swapped = dot(swap_back, acts).astype(BF16)
    dense_swapped = dot(swap_back, dense).astype(BF16)
    part1 = dot(acts_swapped, down[:, half:]) + dot(dense_swapped, dense_down[:, half:])
    o1[...] = part1.astype(BF16).reshape(o1.shape)
    if stop == 6:
        arrived("ep_0", nz, z, r0, r0_send, r0_recv)
        return finish()
    sent += exchange("ep_1", ny, y, lambda p: o1.at[p], r1, r1_send, r1_recv)
    r0[z] = o0[z]
    r1[y] = o1[y]
    arrived("ep_0", nz, z, r0, r0_send, r0_recv)
    if stop == 7:
        arrived("ep_1", ny, y, r1, r1_send, r1_recv)
        return finish()
    whole = added(r0, nz)
    for i in range(ny):
        t0[i] = whole[i * rows : (i + 1) * rows, :].astype(BF16)
    sent += exchange("ep_1", ny, y, lambda p: t0.at[p], s0, s0_send, s0_recv)
    arrived("ep_1", ny, y, r1, r1_send, r1_recv)
    whole = added(r1, ny)
    for i in range(nz):
        t1[i] = whole[i * rows : (i + 1) * rows, :].astype(BF16)
    sent += exchange("ep_0", nz, z, lambda p: t1.at[p], s1, s1_send, s1_recv)
    s0[y] = t0[y]
    s1[z] = t1[z]
    arrived("ep_1", ny, y, s0, s0_send, s0_recv)
    arrived("ep_0", nz, z, s1, s1_send, s1_recv)
    combined = jnp.concatenate([added(s0, ny), added(s1, nz)], axis=1)
    output[...] = (residual.astype(F32) + normalize(combined, out_gain[...])).astype(BF16)
    for copy in sent:
        copy.wait_send()


def tail_kernel(a, b, c, a_out, b_out, c_out):
    a_out[...] = a[...]
    b_out[...] = b[...]
    c_out[...] = c[...]


def in_vmem(count):
    return [pl.BlockSpec(memory_space=pltpu.VMEM)] * count


def in_place(count):
    return [pl.BlockSpec(memory_space=pl.ANY)] * count


def semaphores(*counts):
    return [pltpu.SemaphoreType.DMA((n,)) for n in counts]


def shards(
    sizes,
    stop,
    tokens,
    lengths,
    cache_latent,
    cache_rope,
    attn_gain,
    latent_gain,
    post_gain,
    ffn_gain,
    out_gain,
    w_latent,
    w_rope_key,
    w_query,
    w_absorb_key,
    w_absorb_value,
    w_out,
    routes,
    route_weights,
    w_exp_gate,
    w_exp_up,
    w_exp_down,
    w_dense_gate,
    w_dense_up,
    w_dense_down,
    dense_gate_vector,
):
    rows, width = tokens.shape
    nz, ny, nc, nx = sizes["ep_0"], sizes["ep_1"], sizes["ep_2"], sizes["tp"]
    half = width // 2
    experts = nz * ny * nc
    heads, nope, rank = w_absorb_key.shape
    rope = w_rope_key.shape[1]
    part = w_latent.shape[1]
    floats = part + heads * rope
    inverse = np.float32(rope_base) ** (-np.arange(rope // 2, dtype=np.float32) / (rope // 2))
    inverse = np.concatenate([inverse, inverse])[None]
    V = pltpu.VMEM
    weights = (w_exp_gate, w_exp_up, w_exp_down, w_dense_gate, w_dense_up, w_dense_down)
    outs = (
        jax.ShapeDtypeStruct((rows, width), BF16),
        jax.ShapeDtypeStruct((rows, rank), BF16),
        jax.ShapeDtypeStruct((rows, rope), BF16),
    )
    args = (
        lengths, tokens, jnp.asarray(inverse), attn_gain[None], latent_gain[None], post_gain[None],
        ffn_gain[None], out_gain[None], dense_gate_vector[None], routes, route_weights,
        w_latent.T, w_rope_key.T, w_query.T, w_absorb_key, jnp.swapaxes(w_absorb_value, 1, 2),
        w_out, cache_latent, cache_rope, *weights,
    )
    plane = [ny - 1, ny, nz - 1, nz, nz - 1, nz, ny - 1, ny]
    results = pl.pallas_call(
        functools.partial(layer_kernel, sizes, stop),
        out_shape=outs,
        in_specs=[pl.BlockSpec(memory_space=pltpu.SMEM)] + in_place(len(args) - 1),
        out_specs=tuple(in_vmem(3)),
        scratch_shapes=[
            V((rows, width), BF16),
            V((1, rope), F32),
            V((1, width), F32),
            V((1, rank), F32),
            V((1, width), F32),
            V((1, width), F32),
            V((1, width), F32),
            V((1, width), F32),
            V(routes.shape, jnp.int32),
            V(route_weights.shape, F32),
            V((heads * nope + floats, width), BF16),
            V((rope, width), BF16),
            V(w_absorb_key.shape, BF16),
            V((heads, w_absorb_value.shape[2], rank), BF16),
            V(w_out.shape, BF16),
            V(cache_latent.shape, BF16),
            V(cache_rope.shape, BF16),
            *[V((nc, *w.shape), BF16) for w in weights],
            V((nx, rows, width), BF16),
            V((nx * rows, width), F32),
            V((nx, rows, heads * rank), BF16),
            V((nx, rows, heads * rank), BF16),
            V((nx, rows, floats), F32),
            V((nx, rows, floats), F32),
            V((heads * nope, heads * rank), BF16),
            V((rows, nx * heads, rank), F32),
            V((rows, nx * heads, rope), F32),
            V((nx, rows, heads * rank), F32),
            V((nx, rows, heads * rank), BF16),
            V((nx, rows, heads * rank), BF16),
            V((nx * rows, heads * rank), F32),
            V((nx, rows, width), BF16),
            V((nx, rows, width), BF16),
            V((ny, rows, experts), BF16),
            V((nz, rows, experts), BF16),
            V((ny * rows, experts), F32),
            V((nz * rows, experts), F32),
            V((nz, ny * rows, experts), BF16),
            V((ny, nz * rows, experts), BF16),
            V((ny, rows, half), BF16),
            V((nz, rows, half), BF16),
            V((ny * rows, half), F32),
            V((nz * rows, half), F32),
            V((nz, ny * rows, half), BF16),
            V((ny, nz * rows, half), BF16),
            V((nz, ny * rows, half), BF16),
            V((ny, nz * rows, half), BF16),
            V((nz, ny * rows, half), BF16),
            V((ny, nz * rows, half), BF16),
            V((ny, rows, half), BF16),
            V((nz, rows, half), BF16),
            V((ny, rows, half), BF16),
            V((nz, rows, half), BF16),
        ]
        + semaphores(40, 6, 6, *([nx - 1, nx] * 5), *(plane * 3)),
        compiler_params=pltpu.CompilerParams(collective_id=0, has_side_effects=True),
        name="layer",
    )(*args)
    return pl.pallas_call(
        tail_kernel,
        out_shape=outs,
        in_specs=in_vmem(3),
        out_specs=tuple(in_vmem(3)),
        name="tail",
    )(*results)


def solution(mesh, dims=(8, 8, 2), stop=0):
    torus = Mesh(mesh.devices.reshape(*dims, mesh.shape["tp"]), EP_TP)
    placed = (
        P(EP_TP, None),
        P(EP_TP),
        P(EP_TP, None, None),
        P(EP_TP, None, None),
        P(),
        P(),
        P(),
        P(),
        P(),
        P(None, "tp"),
        P(),
        P(None, "tp"),
        P("tp", None, None),
        P("tp", None, None),
        P("tp", None),
        P(EP_TP, None),
        P(EP_TP, None),
        P(EP, None, None),
        P(EP, None, None),
        P(EP, None, None),
        P(EP, None),
        P(EP, None),
        P(EP, None),
        P(),
    )
    return jax.shard_map(
        functools.partial(shards, dict(torus.shape), stop),
        mesh=torus,
        in_specs=placed,
        out_specs=(P(EP_TP, None), P(EP_TP, None), P(EP_TP, None)),
        check_vma=False,
    )
```

time: 78.5 us -> 65.2 us (0.83)
  the two profiles are of different devices: /device:TPU:16 before, /device:TPU:4 now
where the time goes in v2:
time: 65.2 us; the launch traced here: 65.1 us
  Pallas kernels  64.4 us (99%)
    pallas_call x1, Pallas kernels, shards(): pl.pallas_call(functools.partial(layer_kernel, sizes, stop), out_shape=ou...  63.1 us
    pallas_call x1, Pallas kernels, shards(): pl.pallas_call(tail_kernel, out_shape=outs, in_specs=in_vmem(3), out_spec...  1.31 us

profile of v2, /device:TPU:4, one launch (start us, length us, event | category | flops | bytes accessed | tf_op | source)
XLA Modules:
  0.0 65.1 jit_solution(15233257671358336967)
XLA Ops:
  0.6 63.1 %layer.1 = (bf16[4,1024]{1,0:T(4,128)(2,1)}, bf16[4,256]{1,0:T(4,128)(2,1)}, bf16[4,32]{1,0:T(4,128)(2,1)}) custom-call(s32[4]{0:T(128)} %lengths.1, bf16[4,1024]{1,0:T(4,128)(2,1)} %tokens_in.1, f32[1,32]{1,0:T(1,128)} %constant.2.clone.inverse_in, f32[1,1024]{1,0:T(1,128)} %bitcast.14, f32[1,256]{1,0:T(1,128)} %bitcast.19, f32[1,1024]{1,0:T(1,128)} %bitcast.15, ...), custom_call_target="tpu_custom_call" | custom-call | tf_op jit(solution)/shard_map/layer/pallas_call | solution.py:492
  63.7 1.3 %tail.1 = (bf16[4,1024]{1,0:T(4,128)(2,1)}, bf16[4,256]{1,0:T(4,128)(2,1)}, bf16[4,32]{1,0:T(4,128)(2,1)}) custom-call(bf16[4,1024]{1,0:T(4,128)(2,1)} %get-tuple-element.6.a, bf16[4,256]{1,0:T(4,128)(2,1)} %get-tuple-element.7.b, bf16[4,32]{1,0:T(4,128)(2,1)} %get-tuple-element.8.c), custom_call_target="tpu_custom_call" | custom-call | tf_op jit(solution)/shard_map/tail/pallas_call | solution.py:556

commit v3 on v2

v3 whole, which is shorter than its diff:
```python
import functools

import jax
import jax.numpy as jnp
import numpy as np
from jax import lax
from jax.experimental import pallas as pl
from jax.experimental.pallas import tpu as pltpu
from jax.sharding import Mesh
from jax.sharding import PartitionSpec as P

EP = ("ep_0", "ep_1", "ep_2")
EP_TP = ("ep_0", "ep_1", "ep_2", "tp")
MESH = pl.DeviceIdType.MESH
F32 = jnp.float32
BF16 = jnp.bfloat16

epsilon = 1e-06
rope_base = 10000.0
negative = -1e30


def dot(a, b):
    return jnp.dot(a, b, preferred_element_type=F32)


def dot_nt(a, b):
    return lax.dot_general(a, b, (((1,), (1,)), ((), ())), preferred_element_type=F32)


def normalize(values, gain):
    values = values.astype(F32)
    mean = jnp.mean(values * values, axis=-1, keepdims=True)
    return values * lax.rsqrt(mean + epsilon) * gain


def swap_halves(values):
    half = values.shape[-1] // 2
    return jnp.concatenate([values[:, half:], values[:, :half]], axis=1)


def silu(values):
    return values / (1.0 + jnp.exp(-values))


def exchange(axis, size, me, src_of, dst, send, recv):
    copies = []
    for k in range(1, size):
        partner = lax.rem(me + k, size)
        copy = pltpu.make_async_remote_copy(
            src_ref=src_of(partner),
            dst_ref=dst.at[me],
            send_sem=send.at[k - 1],
            recv_sem=recv.at[me],
            device_id={axis: partner},
            device_id_type=MESH,
        )
        copy.start()
        copies.append(copy)
    return copies


def arrived(axis, size, me, dst, send, recv):
    for k in range(1, size):
        partner = lax.rem(me + k, size)
        pltpu.make_async_remote_copy(
            src_ref=dst.at[partner],
            dst_ref=dst.at[partner],
            send_sem=send.at[k - 1],
            recv_sem=recv.at[partner],
            device_id={axis: partner},
            device_id_type=MESH,
        ).wait_recv()


def offsets(size):
    order = [0]
    for k in range(1, (size + 1) // 2):
        order += [k, -k]
    if size % 2 == 0:
        order.append(size // 2)
    return order, [order.index(-k if -k in order else k) for k in order]


def ring_copy(where, size, off, src, dst, send, recv):
    return pltpu.make_async_remote_copy(
        src_ref=src, dst_ref=dst, send_sem=send, recv_sem=recv,
        device_id=where(off), device_id_type=MESH,
    )


def ring_send(where, size, src_of, dst, send, recv, order):
    offs, back = offsets(size)
    copies = []
    for j in order:
        copy = ring_copy(
            where, size, offs[j], src_of(j), dst.at[back[j]], send.at[j], recv.at[back[j]]
        )
        copy.start()
        copies.append(copy)
    return copies


def ring_wait(where, size, dst, send, recv, order):
    offs, _ = offsets(size)
    for j in order:
        ring_copy(where, size, offs[j], dst.at[j], dst.at[j], send.at[j], recv.at[j]).wait_recv()


def greet(axes):
    barrier = pltpu.get_barrier_semaphore()
    total = 0
    for axis, size in axes:
        me = lax.axis_index(axis)
        for k in range(1, size):
            pl.semaphore_signal(
                barrier,
                inc=1,
                device_id={axis: lax.rem(me + k, size)},
                device_id_type=MESH,
            )
            total += 1
    return barrier, total


def stack_rows(blocks, stack, count, rows):
    for i in range(count):
        stack[i * rows : (i + 1) * rows, :] = blocks[i].astype(F32)
    return stack[...].astype(BF16)


def added(blocks, count):
    total = blocks[0].astype(F32)
    for i in range(1, count):
        total = total + blocks[i].astype(F32)
    return total


def layer_kernel(
    sizes,
    stop,
    lengths, tokens_in, inverse_in, attn_gain_in, latent_gain_in, post_gain_in, ffn_gain_in,
    out_gain_in, gate_vector_in, routes_in, route_weights_in,
    w_latent, w_rope_key, w_query, w_absorb_key, w_absorb_value, w_out,
    cache_latent, cache_rope,
    w_exp_gate, w_exp_up, w_exp_down, w_dense_gate, w_dense_up, w_dense_down,
    output, latent_out, rope_out,
    tokens, inverse, attn_gain, latent_gain, post_gain, ffn_gain, out_gain, gate_vector,
    routes, route_weights, w_front, w_rope, wk, wv, wo, lat, rop, wg, wu, wd, dg, du, dd,
    hid, stack, qmsg_src, qmsg, fmsg_src, fmsg, wk_pad, q_lat, q_rot, lat_rep, rope_rep,
    gw, ws, gat, stack_x, xs, outs, back_in, part_src, parts,
    in_sem, far_send, far_recv,
    hid_send, hid_recv, q_send, q_recv, f_send, f_recv,
    wv_send, wv_recv, wo_send, wo_recv, fv_send, fv_recv, fo_send, fo_recv,
    gw_send, gw_recv, ws_send, ws_recv, g_send, g_recv, x_send, x_recv,
    o_send, o_recv, p_send, p_recv,
):
    nz, ny, nc, nx = sizes["ep_0"], sizes["ep_1"], sizes["ep_2"], sizes["tp"]
    z, y, core = lax.axis_index("ep_0"), lax.axis_index("ep_1"), lax.axis_index("ep_2")
    x = lax.axis_index("tp")
    rows, width = tokens.shape
    experts = nz * ny * nc
    heads, nope, rank = w_absorb_key.shape
    part = w_latent.shape[0]
    rope = w_rope_key.shape[0]
    span = nope + rope
    barrier, total = greet((("tp", nx), ("ep_2", nc), ("ep_1", ny), ("ep_0", nz)))

    moves = [
        (tokens_in, tokens), (attn_gain_in, attn_gain),
        (routes_in, routes), (route_weights_in, route_weights), (inverse_in, inverse),
    ]
    front = [(w_rope_key, w_rope)]
    for h in range(heads):
        front.append((w_query.at[pl.ds(h * span, nope)], w_front.at[pl.ds(h * nope, nope)]))
    front.append((w_latent, w_front.at[pl.ds(heads * nope, part)]))
    for h in range(heads):
        front.append(
            (
                w_query.at[pl.ds(h * span + nope, rope)],
                w_front.at[pl.ds(heads * nope + part + h * rope, rope)],
            )
        )
    front.append((w_absorb_key, wk))
    middle = [
        (latent_gain_in, latent_gain), (cache_latent, lat), (cache_rope, rop),
        (w_absorb_value, wv.at[x]), (w_out, wo.at[x]), (post_gain_in, post_gain), (ffn_gain_in, ffn_gain),
        (out_gain_in, out_gain), (gate_vector_in, gate_vector),
    ]
    pairs = [
        (w_exp_gate, wg), (w_exp_up, wu), (w_exp_down, wd),
        (w_dense_gate, dg), (w_dense_up, du), (w_dense_down, dd),
    ]
    back = [(src, dst.at[core]) for src, dst in pairs]
    started = []
    for src, dst in moves + front + middle + back:
        copy = pltpu.make_async_copy(src, dst, in_sem.at[len(started)])
        copy.start()
        started.append(copy)
    waiting = iter(started)

    def take(count):
        for _ in range(count):
            next(waiting).wait()

    take(len(moves))
    toks = tokens[...].astype(F32)
    hidden = normalize(toks, attn_gain[...]).astype(BF16)
    hid[x] = hidden
    lane = lax.broadcasted_iota(jnp.int32, (rows, experts), 1)
    chosen = routes[...]
    given = route_weights[...]
    spread = jnp.zeros((rows, experts), F32)
    for k in range(routes.shape[1]):
        spread = spread + jnp.where(lane == chosen[:, k : k + 1], given[:, k : k + 1], 0.0)
    gw[0] = spread

    pl.semaphore_wait(barrier, total)
    sent = []

    def finish():
        for copy in waiting:
            copy.wait()
        for copy in sent:
            copy.wait_send()
        output[...] = toks.astype(BF16)

    sent += exchange("tp", nx, x, lambda p: hid.at[x], hid, hid_send, hid_recv)
    other = lax.rem(core + 1, nc)
    share = heads // nc
    mine = pl.ds(core * share, share)
    theirs = pl.ds(other * share, share)

    def weights_along_x(k):
        partner = lax.rem(x + k, nx)
        for src, dst, send, recv in (
            (w_absorb_value, wv, wv_send, wv_recv), (w_out, wo, wo_send, wo_recv)
        ):
            copy = pltpu.make_async_remote_copy(
                src_ref=src.at[mine], dst_ref=dst.at[x, mine],
                send_sem=send.at[k - 1], recv_sem=recv.at[nx - k - 1],
                device_id={"tp": partner}, device_id_type=MESH,
            )
            copy.start()
            sent.append(copy)

    def passed_on(k, start):
        source = lax.rem(x + k, nx)
        for dst, send, recv, far_send_, far_recv_ in (
            (wv, wv_send, wv_recv, fv_send, fv_recv), (wo, wo_send, wo_recv, fo_send, fo_recv)
        ):
            if start:
                pltpu.make_async_remote_copy(
                    src_ref=dst.at[source, mine], dst_ref=dst.at[source, mine],
                    send_sem=send.at[k - 1], recv_sem=recv.at[k - 1],
                    device_id={"tp": source}, device_id_type=MESH,
                ).wait_recv()
                copy = pltpu.make_async_remote_copy(
                    src_ref=dst.at[source, mine], dst_ref=dst.at[source, mine],
                    send_sem=far_send_.at[k - 1], recv_sem=far_recv_.at[k - 1],
                    device_id={"ep_2": other}, device_id_type=MESH,
                )
                copy.start()
                sent.append(copy)
            else:
                pltpu.make_async_remote_copy(
                    src_ref=dst.at[source, theirs], dst_ref=dst.at[source, theirs],
                    send_sem=far_send_.at[k - 1], recv_sem=far_recv_.at[k - 1],
                    device_id={"ep_2": other}, device_id_type=MESH,
                ).wait_recv()

    near_x = [k for k in range(1, nx) if k in (1, nx - 1)]
    far_x = [k for k in range(1, nx) if k not in near_x]
    for k in near_x:
        weights_along_x(k)
    far = [
        pltpu.make_async_remote_copy(
            src_ref=src, dst_ref=dst.at[core], send_sem=far_send.at[i], recv_sem=far_recv.at[i],
            device_id={"ep_2": other}, device_id_type=MESH,
        )
        for i, (src, dst) in enumerate(pairs)
    ]
    for copy in far:
        copy.start()
    ring = ny
    far_first = list(range(ring - 1, 0, -1))

    def along_a(off):
        return {
            "ep_0": lax.rem(z + core * off + ring, ring),
            "ep_1": lax.rem(y + (1 - core) * off + ring, ring),
        }

    def along_b(off):
        return {
            "ep_0": lax.rem(z + (1 - core) * off + ring, ring),
            "ep_1": lax.rem(y + core * off + ring, ring),
        }

    sent += ring_send(along_a, ring, lambda j: gw.at[0], gw, gw_send, gw_recv, far_first)

    total_heads = nx * heads
    all_rows = total_heads * rows
    row = lax.broadcasted_iota(jnp.int32, (all_rows, rope), 0) % rows
    held = jnp.zeros((all_rows, rope), F32)
    for s in range(rows):
        held = jnp.where(row == s, lengths[s].astype(F32), held)
    angles = held * inverse[...]
    cos = jnp.cos(angles)
    sin = jnp.sin(angles)
    first_half = lax.broadcasted_iota(jnp.int32, (all_rows, rope), 1) < rope // 2
    sin = jnp.where(first_half, -sin, sin)
    wk_pad[...] = jnp.zeros(wk_pad.shape, BF16)
    take(len(front))
    for h in range(heads):
        wk_pad[h * nope : (h + 1) * nope, h * rank : (h + 1) * rank] = wk[h]
    rope_pre = dot_nt(hidden, w_rope[...])
    new_rope = (rope_pre * cos[:rows] + swap_halves(rope_pre) * sin[:rows]).astype(BF16)
    rope_out[...] = new_rope
    arrived("tp", nx, x, hid, hid_send, hid_recv)
    projected = dot_nt(stack_rows(hid, stack, nx, rows), w_front[...])
    flat = heads * nope
    query_latent = dot(projected[:, :flat].astype(BF16), wk_pad[...])
    for t in range(nx):
        for h in range(heads):
            qmsg_src[t, h] = query_latent[
                t * rows : (t + 1) * rows, h * rank : (h + 1) * rank
            ].astype(BF16)
        fmsg_src[t] = projected[t * rows : (t + 1) * rows, flat:]
    sent += exchange("tp", nx, x, lambda p: fmsg_src.at[p], fmsg, f_send, f_recv)
    sent += exchange("tp", nx, x, lambda p: qmsg_src.at[p], qmsg, q_send, q_recv)
    for k in far_x:
        weights_along_x(k)
    qmsg[x] = qmsg_src[x]
    fmsg[x] = fmsg_src[x]
    ring_wait(along_a, ring, gw, gw_send, gw_recv, far_first)
    for i in range(ring):
        ws[0, i * rows : (i + 1) * rows, :] = gw[i]
    arrived("tp", nx, x, fmsg, f_send, f_recv)
    pieces = [fmsg[t] for t in range(nx)]
    latent_full = jnp.concatenate([p[:, :part] for p in pieces], axis=1)
    take(len(middle))
    new_latent = normalize(latent_full, latent_gain[...]).astype(BF16)
    latent_out[...] = new_latent
    latent_f = new_latent.astype(F32)
    rope_f = new_rope.astype(F32)
    for t in range(nx):
        values = pieces[t].astype(BF16).astype(F32)
        for h in range(heads):
            at = (t * heads + h) * rows
            q_rot[at : at + rows, :] = values[:, part + h * rope : part + (h + 1) * rope]
            lat_rep[at : at + rows, :] = latent_f
            rope_rep[at : at + rows, :] = rope_f
    arrived("tp", nx, x, qmsg, q_send, q_recv)
    sent += ring_send(along_b, ring, lambda j: ws.at[0], ws, ws_send, ws_recv, far_first)
    for t in range(nx):
        for h in range(heads):
            at = (t * heads + h) * rows
            q_lat[at : at + rows, :] = qmsg[t, h].astype(F32)
    for k in near_x:
        passed_on(k, True)

    def early():
        for copy in far:
            copy.wait()
        ring_wait(along_b, ring, ws, ws_send, ws_recv, far_first)

    if stop == 2:
        for k in far_x:
            passed_on(k, True)
        for k in near_x + far_x:
            passed_on(k, False)
        early()
        return finish()
    scaling = float(span) ** (-0.5)
    cached = lat.shape[1]
    sequence = lax.broadcasted_iota(jnp.int32, (all_rows, cached), 0) % rows
    position = lax.broadcasted_iota(jnp.int32, (all_rows, cached), 1)
    ql_f = q_lat[...]
    ql = ql_f.astype(BF16)
    raw = q_rot[...]
    qr = (raw * cos + swap_halves(raw) * sin).astype(BF16)
    scores = jnp.zeros((all_rows, cached), F32)
    limit = jnp.zeros((all_rows, cached), jnp.int32)
    for s in range(rows):
        scores = jnp.where(sequence == s, dot_nt(ql, lat[s]) + dot(qr, rop[s]), scores)
        limit = jnp.where(sequence == s, lengths[s], limit)
    own = jnp.sum(ql_f * lat_rep[...], axis=-1, keepdims=True)
    own = (own + jnp.sum(qr.astype(F32) * rope_rep[...], axis=-1, keepdims=True)) * scaling
    scores = jnp.where(position < limit, scores * scaling, negative)
    top = jnp.maximum(jnp.max(scores, axis=-1, keepdims=True), own)
    weights = jnp.exp(scores - top)
    own_weight = jnp.exp(own - top)
    whole = jnp.sum(weights, axis=-1, keepdims=True) + own_weight
    probs = weights / whole
    own_prob = (own_weight / whole).astype(BF16).astype(F32)
    got = own_prob * lat_rep[...]
    for s in range(rows):
        got = got + dot(jnp.where(sequence == s, probs, 0.0).astype(BF16), lat[s])
    attended = got.astype(BF16)
    for k in far_x:
        passed_on(k, True)
    for k in near_x + far_x:
        passed_on(k, False)
    v_head = wv.shape[2]
    heads_out = dot_nt(attended, wv[...].reshape(total_heads * v_head, rank))
    of_row = lax.broadcasted_iota(jnp.int32, heads_out.shape, 0) // rows
    of_column = lax.broadcasted_iota(jnp.int32, heads_out.shape, 1) // v_head
    heads_out = jnp.where(of_row == of_column, heads_out, 0.0)
    head_out = heads_out[:rows]
    for n in range(1, total_heads):
        head_out = head_out + heads_out[n * rows : (n + 1) * rows]
    head_out = head_out.astype(BF16)
    group = heads * v_head
    mixed = jnp.zeros((rows, width), F32)
    for t in range(nx):
        piece = dot(head_out[:, t * group : (t + 1) * group], wo[t].reshape(group, width))
        mixed = mixed + piece.astype(BF16).astype(F32)
    if stop == 4:
        early()
        return finish()
    residual = (toks + normalize(mixed, post_gain[...])).astype(BF16)
    ffn_in = normalize(residual, ffn_gain[...]).astype(BF16)

    gat[0] = ffn_in
    sent += ring_send(along_a, ring, lambda j: gat.at[0], gat, g_send, g_recv, far_first)
    early()
    take(len(back))
    ring_wait(along_a, ring, gat, g_send, g_recv, far_first)
    xs[0] = stack_rows(gat, stack_x, ring, rows)
    sent += ring_send(along_b, ring, lambda j: xs.at[0], xs, x_send, x_recv, far_first)
    if stop == 5:
        ring_wait(along_b, ring, xs, x_send, x_recv, far_first)
        return finish()
    block = ring * rows
    chip = (z * ny + y) * nc
    units = nc * dg.shape[1]
    dense_gate = dg[...].reshape(units, width)
    dense_up = du[...].reshape(units, width)
    dense_down = dd[...].reshape(units, width)
    down = wd[...].reshape(nc * wd.shape[2], width)
    for low, high in groups(ring):
        ring_wait(
            along_b, ring, xs, x_send, x_recv, [j for j in range(high - 1, low - 1, -1) if j]
        )
        count = (high - low) * block
        every = xs[low:high].reshape(count, width)
        spread = ws[low:high].reshape(count, experts)
        columns = lax.broadcasted_iota(jnp.int32, (count, experts), 1)
        acts = []
        for e in range(nc):
            share = jnp.sum(jnp.where(columns == chip + e, spread, 0.0), axis=1, keepdims=True)
            act = silu(dot(every, wg[e, 0])) * dot(every, wu[e, 0])
            acts.append((act * share).astype(BF16))
        gate = jnp.sum(every.astype(F32) * gate_vector[...], axis=1, keepdims=True)
        gate = 1.0 / (1.0 + jnp.exp(-gate))
        dense = silu(dot_nt(every, dense_gate)) * dot_nt(every, dense_up)
        dense = (dense * gate).astype(BF16)
        shares = dot(jnp.concatenate(acts, axis=1), down) + dot(dense, dense_down)
        outs[low:high] = shares.astype(BF16).reshape(high - low, block, width)
        sent += ring_send(
            along_b, ring, lambda j: outs.at[j], back_in, o_send, o_recv,
            [j for j in range(high - 1, low - 1, -1) if j],
        )
    if stop == 6:
        ring_wait(along_b, ring, back_in, o_send, o_recv, far_first)
        return finish()
    whole = outs[0].astype(F32)
    for j in far_first:
        ring_wait(along_b, ring, back_in, o_send, o_recv, [j])
        whole = whole + back_in[j].astype(F32)
    for i in range(ring):
        part_src[i] = whole[i * rows : (i + 1) * rows, :].astype(BF16)
    sent += ring_send(along_a, ring, lambda j: part_src.at[j], parts, p_send, p_recv, far_first)
    combined = part_src[0].astype(F32)
    for j in far_first:
        ring_wait(along_a, ring, parts, p_send, p_recv, [j])
        combined = combined + parts[j].astype(F32)
    output[...] = (residual.astype(F32) + normalize(combined, out_gain[...])).astype(BF16)
    for copy in sent:
        copy.wait_send()


def groups(ring):
    if ring == 8:
        return ((5, 8), (3, 5), (0, 3))
    return ((ring // 2, ring), (0, ring // 2))


def tail_kernel(a, b, c, a_out, b_out, c_out):
    a_out[...] = a[...]
    b_out[...] = b[...]
    c_out[...] = c[...]


def in_vmem(count):
    return [pl.BlockSpec(memory_space=pltpu.VMEM)] * count


def in_place(count):
    return [pl.BlockSpec(memory_space=pl.ANY)] * count


def semaphores(*counts):
    return [pltpu.SemaphoreType.DMA((n,)) for n in counts]


def shards(
    sizes,
    stop,
    tokens,
    lengths,
    cache_latent,
    cache_rope,
    attn_gain,
    latent_gain,
    post_gain,
    ffn_gain,
    out_gain,
    w_latent,
    w_rope_key,
    w_query,
    w_absorb_key,
    w_absorb_value,
    w_out,
    routes,
    route_weights,
    w_exp_gate,
    w_exp_up,
    w_exp_down,
    w_dense_gate,
    w_dense_up,
    w_dense_down,
    dense_gate_vector,
):
    rows, width = tokens.shape
    nz, ny, nc, nx = sizes["ep_0"], sizes["ep_1"], sizes["ep_2"], sizes["tp"]
    experts = nz * ny * nc
    heads, nope, rank = w_absorb_key.shape
    rope = w_rope_key.shape[1]
    part = w_latent.shape[1]
    floats = part + heads * rope
    inverse = np.float32(rope_base) ** (-np.arange(rope // 2, dtype=np.float32) / (rope // 2))
    inverse = np.concatenate([inverse, inverse])[None]
    V = pltpu.VMEM
    weights = (w_exp_gate, w_exp_up, w_exp_down, w_dense_gate, w_dense_up, w_dense_down)
    outs = (
        jax.ShapeDtypeStruct((rows, width), BF16),
        jax.ShapeDtypeStruct((rows, rank), BF16),
        jax.ShapeDtypeStruct((rows, rope), BF16),
    )
    args = (
        lengths, tokens, jnp.asarray(inverse), attn_gain[None], latent_gain[None], post_gain[None],
        ffn_gain[None], out_gain[None], dense_gate_vector[None], routes, route_weights,
        w_latent.T, w_rope_key.T, w_query.T, w_absorb_key, jnp.swapaxes(w_absorb_value, 1, 2),
        w_out.reshape(heads, -1, width), cache_latent, cache_rope, *weights,
    )
    results = pl.pallas_call(
        functools.partial(layer_kernel, sizes, stop),
        out_shape=outs,
        in_specs=[pl.BlockSpec(memory_space=pltpu.SMEM)] + in_place(len(args) - 1),
        out_specs=tuple(in_vmem(3)),
        scratch_shapes=[
            V((rows, width), BF16),
            V((1, rope), F32),
            V((1, width), F32),
            V((1, rank), F32),
            V((1, width), F32),
            V((1, width), F32),
            V((1, width), F32),
            V((1, width), F32),
            V(routes.shape, jnp.int32),
            V(route_weights.shape, F32),
            V((heads * nope + floats, width), BF16),
            V((rope, width), BF16),
            V(w_absorb_key.shape, BF16),
            V((nx, heads, w_absorb_value.shape[2], rank), BF16),
            V((nx, heads, w_absorb_value.shape[2], width), BF16),
            V(cache_latent.shape, BF16),
            V(cache_rope.shape, BF16),
            *[V((nc, *w.shape), BF16) for w in weights],
            V((nx, rows, width), BF16),
            V((nx * rows, width), F32),
            V((nx, heads, rows, rank), BF16),
            V((nx, heads, rows, rank), BF16),
            V((nx, rows, floats), F32),
            V((nx, rows, floats), F32),
            V((heads * nope, heads * rank), BF16),
            V((nx * heads * rows, rank), F32),
            V((nx * heads * rows, rope), F32),
            V((nx * heads * rows, rank), F32),
            V((nx * heads * rows, rope), F32),
            V((ny, rows, experts), F32),
            V((ny, ny * rows, experts), F32),
            V((ny, rows, width), BF16),
            V((ny * rows, width), F32),
            V((ny, ny * rows, width), BF16),
            V((ny, ny * rows, width), BF16),
            V((ny, ny * rows, width), BF16),
            V((ny, rows, width), BF16),
            V((ny, rows, width), BF16),
        ]
        + semaphores(40, 6, 6, *([nx - 1, nx] * 3), *([nx - 1] * 8), *([ny] * 12)),
        compiler_params=pltpu.CompilerParams(collective_id=0, has_side_effects=True),
        name="layer",
    )(*args)
    return pl.pallas_call(
        tail_kernel,
        out_shape=outs,
        in_specs=in_vmem(3),
        out_specs=tuple(in_vmem(3)),
        name="tail",
    )(*results)


def solution(mesh, dims=(8, 8, 2), stop=0):
    torus = Mesh(mesh.devices.reshape(*dims, mesh.shape["tp"]), EP_TP)
    placed = (
        P(EP_TP, None),
        P(EP_TP),
        P(EP_TP, None, None),
        P(EP_TP, None, None),
        P(),
        P(),
        P(),
        P(),
        P(),
        P(None, "tp"),
        P(),
        P(None, "tp"),
        P("tp", None, None),
        P("tp", None, None),
        P("tp", None),
        P(EP_TP, None),
        P(EP_TP, None),
        P(EP, None, None),
        P(EP, None, None),
        P(EP, None, None),
        P(EP, None),
        P(EP, None),
        P(EP, None),
        P(),
    )
    return jax.shard_map(
        functools.partial(shards, dict(torus.shape), stop),
        mesh=torus,
        in_specs=placed,
        out_specs=(P(EP_TP, None), P(EP_TP, None), P(EP_TP, None)),
        check_vma=False,
    )
```

time: 65.2 us -> 56 us (0.86)
  the two profiles are of different devices: /device:TPU:4 before, /device:TPU:1 now
where the time goes in v3:
time: 56 us; the launch traced here: 55.8 us
  Pallas kernels  55.2 us (99%)
  between operations  0.65 us (1%)
    pallas_call x1, Pallas kernels, shards(): pl.pallas_call(functools.partial(layer_kernel, sizes, stop), out_shape=ou...  53.9 us
    pallas_call x1, Pallas kernels, shards(): pl.pallas_call(tail_kernel, out_shape=outs, in_specs=in_vmem(3), out_spec...  1.31 us

profile of v3, /device:TPU:1, one launch (start us, length us, event | category | flops | bytes accessed | tf_op | source)
XLA Modules:
  0.0 55.8 jit_solution(18355081690093145591)
XLA Ops:
  0.6 53.9 %layer.1 = (bf16[4,1024]{1,0:T(4,128)(2,1)}, bf16[4,256]{1,0:T(4,128)(2,1)}, bf16[4,32]{1,0:T(4,128)(2,1)}) custom-call(s32[4]{0:T(128)} %lengths.1, bf16[4,1024]{1,0:T(4,128)(2,1)} %tokens_in.1, f32[1,32]{1,0:T(1,128)} %constant.2.clone.inverse_in, f32[1,1024]{1,0:T(1,128)} %bitcast.16, f32[1,256]{1,0:T(1,128)} %bitcast.21, f32[1,1024]{1,0:T(1,128)} %bitcast.17, ...), custom_call_target="tpu_custom_call" | custom-call | tf_op jit(solution)/shard_map/layer/pallas_call | solution.py:558
  54.5 1.3 %tail.1 = (bf16[4,1024]{1,0:T(4,128)(2,1)}, bf16[4,256]{1,0:T(4,128)(2,1)}, bf16[4,32]{1,0:T(4,128)(2,1)}) custom-call(bf16[4,1024]{1,0:T(4,128)(2,1)} %get-tuple-element.6.a, bf16[4,256]{1,0:T(4,128)(2,1)} %get-tuple-element.7.b, bf16[4,32]{1,0:T(4,128)(2,1)} %get-tuple-element.8.c), custom_call_target="tpu_custom_call" | custom-call | tf_op jit(solution)/shard_map/tail/pallas_call | solution.py:607

commit v4 on v3

--- a/solution.py
+++ b/solution.py
@@ -107,20 +107,24 @@
         ring_copy(where, size, offs[j], dst.at[j], dst.at[j], send.at[j], recv.at[j]).wait_recv()
 
 
-def greet(axes):
-    barrier = pltpu.get_barrier_semaphore()
+def tell(semaphore, axes):
     total = 0
-    for axis, size in axes:
+    for axis, distances in axes:
         me = lax.axis_index(axis)
-        for k in range(1, size):
+        for k in distances:
             pl.semaphore_signal(
-                barrier,
+                semaphore,
                 inc=1,
-                device_id={axis: lax.rem(me + k, size)},
+                device_id={axis: lax.rem(me + k, lax.axis_size(axis))},
                 device_id_type=MESH,
             )
             total += 1
-    return barrier, total
+    return total
+
+
+def greet(axes):
+    barrier = pltpu.get_barrier_semaphore()
+    return barrier, tell(barrier, axes)
 
 
 def stack_rows(blocks, stack, count, rows):
@@ -139,17 +143,17 @@
 def layer_kernel(
     sizes,
     stop,
-    lengths, tokens_in, inverse_in, attn_gain_in, latent_gain_in, post_gain_in, ffn_gain_in,
+    lengths_in, tokens_in, inverse_in, attn_gain_in, latent_gain_in, post_gain_in, ffn_gain_in,
     out_gain_in, gate_vector_in, routes_in, route_weights_in,
     w_latent, w_rope_key, w_query, w_absorb_key, w_absorb_value, w_out,
     cache_latent, cache_rope,
     w_exp_gate, w_exp_up, w_exp_down, w_dense_gate, w_dense_up, w_dense_down,
     output, latent_out, rope_out,
-    tokens, inverse, attn_gain, latent_gain, post_gain, ffn_gain, out_gain, gate_vector,
+    lengths, tokens, inverse, attn_gain, latent_gain, post_gain, ffn_gain, out_gain, gate_vector,
     routes, route_weights, w_front, w_rope, wk, wv, wo, lat, rop, wg, wu, wd, dg, du, dd,
     hid, stack, qmsg_src, qmsg, fmsg_src, fmsg, wk_pad, q_lat, q_rot, lat_rep, rope_rep,
     gw, ws, gat, stack_x, xs, outs, back_in, part_src, parts,
-    in_sem, far_send, far_recv,
+    second_sem, fourth_sem, in_sem, far_send, far_recv,
     hid_send, hid_recv, q_send, q_recv, f_send, f_recv,
     wv_send, wv_recv, wo_send, wo_recv, fv_send, fv_recv, fo_send, fo_recv,
     gw_send, gw_recv, ws_send, ws_recv, g_send, g_recv, x_send, x_recv,
@@ -164,10 +168,13 @@
     part = w_latent.shape[0]
     rope = w_rope_key.shape[0]
     span = nope + rope
-    barrier, total = greet((("tp", nx), ("ep_2", nc), ("ep_1", ny), ("ep_0", nz)))
+    ring = ny
+    chained = ring == 8
+    met = (1, ring - 1) if chained else tuple(range(1, ring))
+    barrier, total = greet((("tp", range(1, nx)), ("ep_2", range(1, nc)), ("ep_1", met), ("ep_0", met)))
 
     moves = [
-        (tokens_in, tokens), (attn_gain_in, attn_gain),
+        (lengths_in, lengths), (tokens_in, tokens), (attn_gain_in, attn_gain),
         (routes_in, routes), (route_weights_in, route_weights), (inverse_in, inverse),
     ]
     front = [(w_rope_key, w_rope)]
@@ -216,6 +223,8 @@
     gw[0] = spread
 
     pl.semaphore_wait(barrier, total)
+    if chained:
+        heard = tell(second_sem, (("ep_1", met), ("ep_0", met)))
     sent = []
 
     def finish():
@@ -282,7 +291,6 @@
     ]
     for copy in far:
         copy.start()
-    ring = ny
     far_first = list(range(ring - 1, 0, -1))
 
     def along_a(off):
@@ -297,7 +305,6 @@
             "ep_1": lax.rem(y + core * off + ring, ring),
         }
 
-    sent += ring_send(along_a, ring, lambda j: gw.at[0], gw, gw_send, gw_recv, far_first)
 
     total_heads = nx * heads
     all_rows = total_heads * rows
@@ -317,6 +324,9 @@
     rope_pre = dot_nt(hidden, w_rope[...])
     new_rope = (rope_pre * cos[:rows] + swap_halves(rope_pre) * sin[:rows]).astype(BF16)
     rope_out[...] = new_rope
+    if chained:
+        pl.semaphore_wait(second_sem, heard)
+        heard = tell(fourth_sem, (("ep_1", (2, 6)), ("ep_0", (2, 6))))
     arrived("tp", nx, x, hid, hid_send, hid_recv)
     projected = dot_nt(stack_rows(hid, stack, nx, rows), w_front[...])
     flat = heads * nope
@@ -333,9 +343,9 @@
         weights_along_x(k)
     qmsg[x] = qmsg_src[x]
     fmsg[x] = fmsg_src[x]
-    ring_wait(along_a, ring, gw, gw_send, gw_recv, far_first)
-    for i in range(ring):
-        ws[0, i * rows : (i + 1) * rows, :] = gw[i]
+    if chained:
+        pl.semaphore_wait(fourth_sem, heard)
+    sent += ring_send(along_a, ring, lambda j: gw.at[0], gw, gw_send, gw_recv, far_first)
     arrived("tp", nx, x, fmsg, f_send, f_recv)
     pieces = [fmsg[t] for t in range(nx)]
     latent_full = jnp.concatenate([p[:, :part] for p in pieces], axis=1)
@@ -352,7 +362,6 @@
             lat_rep[at : at + rows, :] = latent_f
             rope_rep[at : at + rows, :] = rope_f
     arrived("tp", nx, x, qmsg, q_send, q_recv)
-    sent += ring_send(along_b, ring, lambda j: ws.at[0], ws, ws_send, ws_recv, far_first)
     for t in range(nx):
         for h in range(heads):
             at = (t * heads + h) * rows
@@ -365,13 +374,6 @@
             copy.wait()
         ring_wait(along_b, ring, ws, ws_send, ws_recv, far_first)
 
-    if stop == 2:
-        for k in far_x:
-            passed_on(k, True)
-        for k in near_x + far_x:
-            passed_on(k, False)
-        early()
-        return finish()
     scaling = float(span) ** (-0.5)
     cached = lat.shape[1]
     sequence = lax.broadcasted_iota(jnp.int32, (all_rows, cached), 0) % rows
@@ -398,6 +400,10 @@
     for s in range(rows):
         got = got + dot(jnp.where(sequence == s, probs, 0.0).astype(BF16), lat[s])
     attended = got.astype(BF16)
+    ring_wait(along_a, ring, gw, gw_send, gw_recv, far_first)
+    for i in range(ring):
+        ws[0, i * rows : (i + 1) * rows, :] = gw[i]
+    sent += ring_send(along_b, ring, lambda j: ws.at[0], ws, ws_send, ws_recv, far_first)
     for k in far_x:
         passed_on(k, True)
     for k in near_x + far_x:
@@ -483,7 +489,7 @@
 
 def groups(ring):
     if ring == 8:
-        return ((5, 8), (3, 5), (0, 3))
+        return ((0, 1), (7, 8), (5, 7), (3, 5), (1, 3))
     return ((ring // 2, ring), (0, ring // 2))
 
 
@@ -558,9 +564,10 @@
     results = pl.pallas_call(
         functools.partial(layer_kernel, sizes, stop),
         out_shape=outs,
-        in_specs=[pl.BlockSpec(memory_space=pltpu.SMEM)] + in_place(len(args) - 1),
+        in_specs=in_place(len(args)),
         out_specs=tuple(in_vmem(3)),
         scratch_shapes=[
+            pltpu.SMEM(lengths.shape, jnp.int32),
             V((rows, width), BF16),
             V((1, rope), F32),
             V((1, width), F32),
@@ -600,6 +607,7 @@
             V((ny, rows, width), BF16),
             V((ny, rows, width), BF16),
         ]
+        + [pltpu.SemaphoreType.REGULAR] * 2
         + semaphores(40, 6, 6, *([nx - 1, nx] * 3), *([nx - 1] * 8), *([ny] * 12)),
         compiler_params=pltpu.CompilerParams(collective_id=0, has_side_effects=True),
         name="layer",

time: 56 us -> 53.4 us (0.954)
  Pallas kernels: 55.2 us -> 52.2 us
    pallas_call x1, Pallas kernels: 53.9 us -> 50.9 us  [shards(): pl.pallas_call(functools.partial(layer_kernel, sizes, stop), out_shape=ou...]
where the time goes in v4:
time: 53.4 us; the launch traced here: 52.9 us
  Pallas kernels  52.2 us (98%)
  between operations  0.65 us (1%)
    pallas_call x1, Pallas kernels, shards(): pl.pallas_call(functools.partial(layer_kernel, sizes, stop), out_shape=ou...  50.9 us
    pallas_call x1, Pallas kernels, shards(): pl.pallas_call(tail_kernel, out_shape=outs, in_specs=in_vmem(3), out_spec...  1.31 us

profile of v4, /device:TPU:1, one launch (start us, length us, event | category | flops | bytes accessed | tf_op | source)
XLA Modules:
  0.0 52.9 jit_solution(3434994699040018891)
XLA Ops:
  0.6 50.9 %layer.1 = (bf16[4,1024]{1,0:T(4,128)(2,1)}, bf16[4,256]{1,0:T(4,128)(2,1)}, bf16[4,32]{1,0:T(4,128)(2,1)}) custom-call(s32[4]{0:T(128)} %lengths_in.1, bf16[4,1024]{1,0:T(4,128)(2,1)} %tokens_in.1, f32[1,32]{1,0:T(1,128)} %constant.2.clone.inverse_in, f32[1,1024]{1,0:T(1,128)} %bitcast.16, f32[1,256]{1,0:T(1,128)} %bitcast.21, f32[1,1024]{1,0:T(1,128)} %bitcast.17, ...), custom_call_target="tpu_custom_call" | custom-call | tf_op jit(solution)/shard_map/layer/pallas_call | solution.py:564
  51.6 1.3 %tail.1 = (bf16[4,1024]{1,0:T(4,128)(2,1)}, bf16[4,256]{1,0:T(4,128)(2,1)}, bf16[4,32]{1,0:T(4,128)(2,1)}) custom-call(bf16[4,1024]{1,0:T(4,128)(2,1)} %get-tuple-element.6.a, bf16[4,256]{1,0:T(4,128)(2,1)} %get-tuple-element.7.b, bf16[4,32]{1,0:T(4,128)(2,1)} %get-tuple-element.8.c), custom_call_target="tpu_custom_call" | custom-call | tf_op jit(solution)/shard_map/tail/pallas_call | solution.py:615

commit v5 on v4

--- a/solution.py
+++ b/solution.py
@@ -293,13 +293,13 @@
         copy.start()
     far_first = list(range(ring - 1, 0, -1))
 
-    def along_a(off):
+    def along_b(off):
         return {
             "ep_0": lax.rem(z + core * off + ring, ring),
             "ep_1": lax.rem(y + (1 - core) * off + ring, ring),
         }
 
-    def along_b(off):
+    def along_a(off):
         return {
             "ep_0": lax.rem(z + (1 - core) * off + ring, ring),
             "ep_1": lax.rem(y + core * off + ring, ring),
@@ -563,7 +563,7 @@
     )
     results = pl.pallas_call(
         functools.partial(layer_kernel, sizes, stop),
-        out_shape=outs,
+        out_shape=tuple(V(o.shape, o.dtype) for o in outs),
         in_specs=in_place(len(args)),
         out_specs=tuple(in_vmem(3)),
         scratch_shapes=[
@@ -618,7 +618,7 @@
         in_specs=in_vmem(3),
         out_specs=tuple(in_vmem(3)),
         name="tail",
-    )(*results)
+    )(*[pltpu.with_memory_space_constraint(r, pltpu.VMEM) for r in results])
 
 
 def solution(mesh, dims=(8, 8, 2), stop=0):

time: 53.4 us -> 51.8 us (0.970)
  Pallas kernels: 52.2 us -> 50.6 us
    pallas_call x1, Pallas kernels: 50.9 us -> 50 us  [shards(): pl.pallas_call(functools.partial(layer_kernel, sizes, stop), out_shape=tu...]
    pallas_call x1, Pallas kernels: 1.31 us -> 0.61 us  [shards(): pl.pallas_call(tail_kernel, out_shape=outs, in_specs=in_vmem(3), out_spec...]
where the time goes in v5:
time: 51.8 us; the launch traced here: 51.3 us
  Pallas kernels  50.6 us (98%)
  between operations  0.65 us (1%)
    pallas_call x1, Pallas kernels, shards(): pl.pallas_call(functools.partial(layer_kernel, sizes, stop), out_shape=tu...  50 us

profile of v5, /device:TPU:1, one launch (start us, length us, event | category | flops | bytes accessed | tf_op | source)
XLA Modules:
  0.0 51.3 jit_solution(10583466643200390610)
XLA Ops:
  0.6 50.0 %layer.1 = (bf16[4,1024]{1,0:T(4,128)(2,1)S(1)}, bf16[4,256]{1,0:T(4,128)(2,1)S(1)}, bf16[4,32]{1,0:T(4,128)(2,1)S(1)}) custom-call(s32[4]{0:T(128)} %lengths_in.1, bf16[4,1024]{1,0:T(4,128)(2,1)} %tokens_in.1, f32[1,32]{1,0:T(1,128)} %constant.2.clone.inverse_in, f32[1,1024]{1,0:T(1,128)} %bitcast.16, f32[1,256]{1,0:T(1,128)} %bitcast.21, ...), custom_call_target="tpu_custom_call" | custom-call | tf_op jit(solution)/shard_map/layer/pallas_call | solution.py:564
  50.7 0.6 %tail.1 = (bf16[4,1024]{1,0:T(4,128)(2,1)}, bf16[4,256]{1,0:T(4,128)(2,1)}, bf16[4,32]{1,0:T(4,128)(2,1)}) custom-call(bf16[4,1024]{1,0:T(4,128)(2,1)S(1)} %get-tuple-element.6.a, bf16[4,256]{1,0:T(4,128)(2,1)S(1)} %get-tuple-element.7.b, bf16[4,32]{1,0:T(4,128)(2,1)S(1)} %get-tuple-element.8.c), custom_call_target="tpu_custom_call" | custom-call | tf_op jit(solution)/shard_map/tail/pallas_call | solution.py:615

commit v6 on v5

--- a/solution.py
+++ b/solution.py
@@ -400,10 +400,6 @@
     for s in range(rows):
         got = got + dot(jnp.where(sequence == s, probs, 0.0).astype(BF16), lat[s])
     attended = got.astype(BF16)
-    ring_wait(along_a, ring, gw, gw_send, gw_recv, far_first)
-    for i in range(ring):
-        ws[0, i * rows : (i + 1) * rows, :] = gw[i]
-    sent += ring_send(along_b, ring, lambda j: ws.at[0], ws, ws_send, ws_recv, far_first)
     for k in far_x:
         passed_on(k, True)
     for k in near_x + far_x:
@@ -422,22 +418,20 @@
     for t in range(nx):
         piece = dot(head_out[:, t * group : (t + 1) * group], wo[t].reshape(group, width))
         mixed = mixed + piece.astype(BF16).astype(F32)
-    if stop == 4:
-        early()
-        return finish()
     residual = (toks + normalize(mixed, post_gain[...])).astype(BF16)
     ffn_in = normalize(residual, ffn_gain[...]).astype(BF16)
 
     gat[0] = ffn_in
     sent += ring_send(along_a, ring, lambda j: gat.at[0], gat, g_send, g_recv, far_first)
-    early()
+    ring_wait(along_a, ring, gw, gw_send, gw_recv, far_first)
+    for i in range(ring):
+        ws[0, i * rows : (i + 1) * rows, :] = gw[i]
+    sent += ring_send(along_b, ring, lambda j: ws.at[0], ws, ws_send, ws_recv, far_first)
     take(len(back))
     ring_wait(along_a, ring, gat, g_send, g_recv, far_first)
     xs[0] = stack_rows(gat, stack_x, ring, rows)
     sent += ring_send(along_b, ring, lambda j: xs.at[0], xs, x_send, x_recv, far_first)
-    if stop == 5:
-        ring_wait(along_b, ring, xs, x_send, x_recv, far_first)
-        return finish()
+    early()
     block = ring * rows
     chip = (z * ny + y) * nc
     units = nc * dg.shape[1]

time: 51.8 us -> 52.6 us (1.015)
  the two profiles are of different devices: /device:TPU:1 before, /device:TPU:8 now
where the time goes in v6:
time: 52.6 us; the launch traced here: 52.5 us
  Pallas kernels  51.8 us (98%)
  between operations  0.65 us (1%)
    pallas_call x1, Pallas kernels, shards(): pl.pallas_call(functools.partial(layer_kernel, sizes, stop), out_shape=tu...  51.2 us

profile of v6, /device:TPU:8, one launch (start us, length us, event | category | flops | bytes accessed | tf_op | source)
XLA Modules:
  0.0 52.5 jit_solution(3306862045678071743)
XLA Ops:
  0.6 51.2 %layer.1 = (bf16[4,1024]{1,0:T(4,128)(2,1)S(1)}, bf16[4,256]{1,0:T(4,128)(2,1)S(1)}, bf16[4,32]{1,0:T(4,128)(2,1)S(1)}) custom-call(s32[4]{0:T(128)} %lengths_in.1, bf16[4,1024]{1,0:T(4,128)(2,1)} %tokens_in.1, f32[1,32]{1,0:T(1,128)} %constant.2.clone.inverse_in, f32[1,1024]{1,0:T(1,128)} %bitcast.16, f32[1,256]{1,0:T(1,128)} %bitcast.21, ...), custom_call_target="tpu_custom_call" | custom-call | tf_op jit(solution)/shard_map/layer/pallas_call | solution.py:558
  51.9 0.6 %tail.1 = (bf16[4,1024]{1,0:T(4,128)(2,1)}, bf16[4,256]{1,0:T(4,128)(2,1)}, bf16[4,32]{1,0:T(4,128)(2,1)}) custom-call(bf16[4,1024]{1,0:T(4,128)(2,1)S(1)} %get-tuple-element.6.a, bf16[4,256]{1,0:T(4,128)(2,1)S(1)} %get-tuple-element.7.b, bf16[4,32]{1,0:T(4,128)(2,1)S(1)} %get-tuple-element.8.c), custom_call_target="tpu_custom_call" | custom-call | tf_op jit(solution)/shard_map/tail/pallas_call | solution.py:609
